TPU v7x, 32 devices: a whole 2x2x4 slice. The times are simulated.
32 devices in a mesh: kv: 8 (over z, y), tp: 4 (over x, core).
Axes of the slice: x: 2, y: 2, z: 4, core: 2. Of those that a mesh axis runs over, the one named last changes fastest.
Arguments:
- tokens: bfloat16 [256, 4096], P(None, ('kv', 'tp')), may hold values from -60 to 60
- past_state: float32 [256, 16, 128, 128], P('kv', 'tp'), may hold values from -4 to 4
- pre_gain: float32 [4096], replicated, may hold values from 0.1 to 1.9
- pre_gate: bfloat16 [4096, 11264], P(None, ('kv', 'tp')), may hold values from -0.09375 to 0.09375
- pre_up: bfloat16 [4096, 11264], P(None, ('kv', 'tp')), may hold values from -0.09375 to 0.09375
- pre_down: bfloat16 [11264, 4096], P(('kv', 'tp')), may hold values from -0.109375 to 0.109375
- mix_gain: float32 [4096], replicated, may hold values from 0.1 to 1.9
- query_weight: bfloat16 [4096, 2048], P('kv', 'tp'), may hold values from -0.09375 to 0.09375
- forget_weight: bfloat16 [4096, 2048], P('kv', 'tp'), may hold values from -0.09375 to 0.09375
- value_weight: bfloat16 [4096, 2048], P('kv', 'tp'), may hold values from -0.09375 to 0.09375
- output_gate_weight: bfloat16 [4096, 2048], P('kv', 'tp'), may hold values from -0.09375 to 0.09375
- forget_floor: float32 [2048], P('tp'), may hold values from 0.02 to 0.9
- head_gain: float32 [128], replicated, may hold values from 0.1 to 1.9
- proj_out: bfloat16 [2048, 4096], P('tp', 'kv'), may hold values from -0.125 to 0.125
- post_gain: float32 [4096], replicated, may hold values from 0.1 to 1.9
- post_gate: bfloat16 [4096, 11264], P(None, ('kv', 'tp')), may hold values from -0.09375 to 0.09375
- post_up: bfloat16 [4096, 11264], P(None, ('kv', 'tp')), may hold values from -0.09375 to 0.09375
- post_down: bfloat16 [11264, 4096], P(('kv', 'tp')), may hold values from -0.109375 to 0.109375
Outputs:
- result: bfloat16 [256, 4096], P(None, ('kv', 'tp'))
- new_state: float32 [256, 16, 128, 128], P('kv', 'tp')
All inputs are finite; a program needn't handle non-finite values.
Results may differ from a plain program's by a relative error of at most 0.014.
Values may be sent and summed in bfloat16 or wider, within the bound.
No kernel may reach another device: no remote copies, remote signals or barrier semaphores. Data moves between devices by JAX's collectives and lax.ppermute only.
A program may use at most 128 MiB of HBM per device.

v0:
```python
import jax
import jax.numpy as jnp
from jax import lax
from jax.sharding import PartitionSpec as P

D = 4096


epsilon = 1e-06


def half_inputs(activations, gain, w_gate, w_up):
    piece_float = lax.all_gather(activations, ("kv", "tp"), axis=1, tiled=True).astype(jnp.float32)
    normed = (piece_float * gain).astype(jnp.bfloat16)
    gate_acc = jnp.dot(normed, w_gate, preferred_element_type=jnp.float32)
    up_acc = jnp.dot(normed, w_up, preferred_element_type=jnp.float32)
    squares = jnp.sum(piece_float * piece_float, axis=1)
    row_scale = lax.rsqrt(squares / D + epsilon)[:, None]
    return (jax.nn.silu(row_scale * gate_acc) * (row_scale * up_acc)).astype(jnp.bfloat16)


def down_sum(hidden, w_down):
    return lax.psum_scatter(
        jnp.dot(hidden, w_down, preferred_element_type=jnp.float32),
        ("kv", "tp"),
        scatter_dimension=1,
        tiled=True,
    )


def per_device(
    tokens,
    past_state,
    pre_gain,
    pre_gate,
    pre_up,
    pre_down,
    mix_gain,
    query_weight,
    forget_weight,
    value_weight,
    output_gate_weight,
    forget_floor,
    head_gain,
    proj_out,
    post_gain,
    post_gate,
    post_up,
    post_down,
):
    whole_rows = lax.all_gather(tokens, ("kv", "tp"), axis=1, tiled=True)
    whole_float = whole_rows.astype(jnp.float32)
    row_scale = lax.rsqrt(jnp.mean(whole_float * whole_float, axis=1, keepdims=True) + epsilon)
    normed = (whole_float * pre_gain).astype(jnp.bfloat16)
    gate_pre = row_scale * jnp.dot(normed, pre_gate, preferred_element_type=jnp.float32)
    up_pre = row_scale * jnp.dot(normed, pre_up, preferred_element_type=jnp.float32)
    hidden = (jax.nn.silu(gate_pre) * up_pre).astype(jnp.bfloat16)
    kv_sums = lax.psum_scatter(
        jnp.dot(hidden, pre_down, preferred_element_type=jnp.float32).astype(jnp.bfloat16),
        "kv",
        scatter_dimension=1,
        tiled=True,
    )
    block_sum = lax.psum(kv_sums, "tp").astype(jnp.float32)
    block_width = block_sum.shape[1]
    block_old = lax.dynamic_slice_in_dim(
        whole_rows, lax.axis_index("kv") * block_width, block_width, 1
    )
    block_rows = (block_old.astype(jnp.float32) + 0.5 * block_sum).astype(jnp.bfloat16)
    own_width = block_width // lax.axis_size("tp")
    after_first = lax.dynamic_slice_in_dim(
        block_rows, lax.axis_index("tp") * own_width, own_width, 1
    )
    block_width = block_rows.shape[1]
    block_float = block_rows.astype(jnp.float32)
    block_gain = lax.dynamic_slice_in_dim(
        mix_gain, lax.axis_index("kv") * block_width, block_width, 0
    )
    squares = lax.psum(jnp.sum(block_float * block_float, axis=1), "kv")
    normed = (block_float * block_gain).astype(jnp.bfloat16)
    own_rows = past_state.shape[0]
    weight_list = (query_weight, forget_weight, value_weight, output_gate_weight)
    projected = lax.psum_scatter(
        jnp.concatenate(
            [
                jnp.dot(normed, weight_part, preferred_element_type=jnp.float32)
                for weight_part in weight_list
            ],
            axis=1,
        ).astype(jnp.bfloat16),
        "kv",
        scatter_dimension=0,
        tiled=True,
    ).astype(jnp.float32)
    own_squares = lax.dynamic_slice_in_dim(squares, lax.axis_index("kv") * own_rows, own_rows, 0)
    projected = projected * lax.rsqrt(own_squares / D + epsilon)[:, None]
    pre_query, pre_forget, pre_value, pre_gate_out = jnp.split(projected, 4, axis=1)
    local_heads = past_state.shape[1]
    head_width = past_state.shape[2]
    head_shape = (own_rows, local_heads, head_width)
    floors = forget_floor.reshape(local_heads, head_width)
    forget_heads = pre_forget.reshape(head_shape)
    forget = floors + (1.0 - floors) * jax.nn.sigmoid(forget_heads)
    written = (1.0 - floors) * jax.nn.sigmoid(-forget_heads)
    query_act = jax.nn.silu(pre_query.reshape(head_shape))
    value_act = pre_value.reshape(head_shape)
    new_state = (
        forget[:, :, :, None] * past_state + written[:, :, :, None] * value_act[:, :, None, :]
    )
    readout = jnp.einsum("bhkv,bhk->bhv", new_state, query_act, precision=lax.Precision.HIGHEST)
    readout = (
        readout
        * lax.rsqrt(jnp.mean(readout * readout, axis=2, keepdims=True) + epsilon)
        * head_gain
    )
    mixed_in = (
        readout.reshape(own_rows, local_heads * head_width) * jax.nn.silu(pre_gate_out)
    ).astype(jnp.bfloat16)
    partials = jnp.dot(
        lax.all_gather(mixed_in, "kv", axis=0, tiled=True),
        proj_out,
        preferred_element_type=jnp.float32,
    ).astype(jnp.bfloat16)
    mixed_sum = lax.psum_scatter(partials, "tp", scatter_dimension=1, tiled=True).astype(
        jnp.float32
    )
    second = (after_first.astype(jnp.float32) + mixed_sum).astype(jnp.bfloat16)
    hidden_two = half_inputs(second, post_gain, post_gate, post_up)
    result = (second.astype(jnp.float32) + 0.5 * down_sum(hidden_two, post_down)).astype(
        jnp.bfloat16
    )
    return (result, new_state)


def solution(mesh):
    placed = (
        P(None, ("kv", "tp")),
        P("kv", "tp", None, None),
        P(),
        P(None, ("kv", "tp")),
        P(None, ("kv", "tp")),
        P(("kv", "tp"), None),
        P(),
        P("kv", "tp"),
        P("kv", "tp"),
        P("kv", "tp"),
        P("kv", "tp"),
        P("tp"),
        P(),
        P("tp", "kv"),
        P(),
        P(None, ("kv", "tp")),
        P(None, ("kv", "tp")),
        P(("kv", "tp"), None),
    )
    return jax.shard_map(
        per_device,
        mesh=mesh,
        in_specs=placed,
        out_specs=(P(None, ("kv", "tp")), P("kv", "tp", None, None)),
        check_vma=False,
    )
```

profile of v0, /device:TPU:0, one launch (start us, length us, event | category | flops | bytes accessed | tf_op | source)
XLA Modules:
  0.0 548.7 jit_solution(15226853268982632663)
XLA Ops:
  8.0 58.6 %all-gather.3.cloned.1.call-done = bf16[256,4096]{1,0:T(8,128)(2,1)} async-done(((bf16[256,128]{1,0:T(8,128)(2,1)}), bf16[256,4096]{1,0:T(8,128)(2,1)}) %all-gather.3.cloned.1.call-update) | async-done | bytes 2097168 | tf_op jit(solution)/shard_map/all_gather | solution.py:51
  66.6 2.1 fusion
  68.7 3.4 fusion.12
  72.1 7.5 %convolution_convert_fusion = bf16[256,4096]{1,0:T(8,128)(2,1)} fusion(bf16[352,4096]{1,0:T(8,128)(2,1)S(1)} %copy-done, bf16[4096,352]{0,1:T(8,128)(2,1)} %param.22, bf16[256,4096]{1,0:T(8,128)(2,1)} %all-gather.3.cloned.1.call-done, f32[4096]{0:T(1024)S(1)} %copy-done.7, f32[256,352]{0,1:T(8,128)S(1)} %fusion.12, f32[256]{0:T(256)S(1)} %add_rsqrt_fusion.2), kind=kOutput, calls=%fused_computation.5 | convolution fusion | flops 1481220096 | bytes 10339328 | tf_op jit(solution)/shard_map/dot_general | solution.py:59
  79.7 68.1 %reduce-scatter.7.cloned.1.call-done = bf16[256,512]{1,0:T(8,128)(2,1)} async-done(((bf16[256,4096]{1,0:T(8,128)(2,1)}), bf16[256,512]{1,0:T(8,128)(2,1)}) %reduce-scatter.7.cloned.1.call-update) | async-done | bytes 262160 | tf_op jit(solution)/shard_map/reduce_scatter | solution.py:58
  148.6 32.8 %all-reduce.2.cloned.1.call-done = bf16[256,512]{1,0:T(8,128)(2,1)} async-done(((bf16[256,512]{1,0:T(8,128)(2,1)}), bf16[256,512]{1,0:T(8,128)(2,1)}) %all-reduce.2.cloned.1.call-update) | async-done | bytes 262160 | tf_op jit(solution)/shard_map/psum | solution.py:64
  181.4 1.2 fusion.42
  182.6 1.3 convolution_convert_fusion.3
  183.9 1.3 convolution_convert_fusion.2
  185.3 1.3 convolution_convert_fusion.4
  186.6 1.3 convolution_convert_fusion.5
  189.2 21.6 %psum.15 = f32[256]{0:T(256)S(1)} all-reduce(f32[256]{0:T(256)S(1)} %get-tuple-element.2), channel_id=1, replica_groups=mesh['kv'=8,'tp'=4] {'kv'}, use_global_device_ids=true, to_apply=%region_5.6 | all-reduce | flops 256 | bytes 2048 | tf_op jit(solution)/shard_map/psum | solution.py:79
  210.8 42.6 %reduce-scatter.9.cloned.1.call-done = bf16[32,2048]{1,0:T(8,128)(2,1)} async-done(((bf16[256,2048]{1,0:T(8,128)(2,1)}), bf16[32,2048]{1,0:T(8,128)(2,1)}) %reduce-scatter.9.cloned.1.call-update) | async-done | bytes 131088 | tf_op jit(solution)/shard_map/reduce_scatter | solution.py:83
  258.2 1.5 div.63
  260.5 8.2 %multiply_add_fusion = f32[32,4,128,128]{3,2,1,0:T(8,128)S(1)} fusion(f32[32,4,128,128]{3,2,1,0:T(8,128)} %param.19, f32[32,4,128]{2,1,0:T(4,128)S(1)} %mul.203, f32[32,4,128]{2,1,0:T(4,128)S(1)} %bitcast.39, f32[32,4,128]{2,1,0:T(4,128)S(1)} %bitcast.38), kind=kLoop, calls=%fused_computation | loop fusion | flops 6291456 | bytes 16973824 | tf_op jit(solution)/shard_map/add | solution.py:108
  268.8 7.2 %fusion.65 = f32[32,4,1,128]{3,2,1,0:T(1,128)S(1)} fusion(f32[32,4,128,128]{3,2,1,0:T(8,128)S(1)} %multiply_add_fusion, f32[32,4,128,1]{2,3,1,0:T(1,128)S(1)} %bitcast.37), kind=kOutput, calls=%fused_computation.68 | convolution fusion | flops 25165824 | bytes 8519680 | tf_op jit(solution)/shard_map/bhkv,bhk->bhv/dot_general | solution.py:110
  276.3 30.8 %all_gather.10 = bf16[256,512]{1,0:T(8,128)(2,1)S(1)} all-gather(bf16[32,512]{1,0:T(8,128)(2,1)S(1)} %fusion.61), channel_id=1, replica_groups=mesh['kv'=8,'tp'=4] {'kv'}, dimensions={0}, use_global_device_ids=true | all-gather | bytes 294912 | tf_op jit(solution)/shard_map/all_gather | solution.py:120
  308.3 19.2 %reduce-scatter.13.cloned.1.call-done = bf16[128,256]{1,0:T(8,128)(2,1)} async-done(((bf16[512,256]{1,0:T(8,128)(2,1)}), bf16[128,256]{1,0:T(8,128)(2,1)}) %reduce-scatter.13.cloned.1.call-update) | async-done | bytes 65552
  329.4 54.4 %all-gather.5.cloned.1.call-done = bf16[256,4096]{1,0:T(8,128)(2,1)} async-done(((bf16[256,128]{1,0:T(8,128)(2,1)}), bf16[256,4096]{1,0:T(8,128)(2,1)}) %all-gather.5.cloned.1.call-update) | async-done | bytes 2097168 | tf_op jit(solution)/shard_map/all_gather | solution.py:13
  383.8 2.1 fusion.2
  385.9 3.4 fusion.18
  389.3 8.9 %fusion.37 = f32[256,4096]{1,0:T(8,128)} fusion(bf16[352,4096]{1,0:T(8,128)(2,1)} %param.35, bf16[4096,352]{0,1:T(8,128)(2,1)} %param.34, bf16[256,4096]{1,0:T(8,128)(2,1)} %all-gather.5.cloned.1.call-done, f32[4096]{0:T(1024)S(1)} %copy-done.4, f32[256,352]{0,1:T(8,128)S(1)} %fusion.18, f32[256]{0:T(256)S(1)} %add_rsqrt_fusion.1), kind=kOutput, calls=%fused_computation.27 | convolution fusion | flops 1480171520 | bytes 12436480 | tf_op jit(solution)/shard_map/dot_general | solution.py:24
  398.3 142.1 %reduce-scatter.11.cloned.1.call-done = f32[256,128]{1,0:T(8,128)} async-done(((f32[256,4096]{1,0:T(8,128)}), f32[256,128]{1,0:T(8,128)}) %reduce-scatter.11.cloned.1.call-update) | async-done | bytes 131088 | tf_op jit(solution)/shard_map/reduce_scatter | solution.py:23
  540.3 1.6 add_convert_fusion.1
  (53 shorter events, 11.8 us)
Async XLA Ops:
  7.2 65.0 %copy-start = (bf16[352,4096]{1,0:T(8,128)(2,1)S(1)}, bf16[352,4096]{1,0:T(8,128)(2,1)}, u32[]{:S(2)}) copy-start(bf16[352,4096]{1,0:T(8,128)(2,1)} %param.23) | copy-start | bytes 8650756
  7.2 59.4 %all-gather.3.cloned.1.call-start = ((), (), s32[]{:S(2)}) async-start(), calls=%async_computation.4 | async-start | bytes 2162688 | tf_op jit(solution)/shard_map/all_gather | solution.py:51
  7.9 139.8 %reduce-scatter.7.cloned.1.call-start = ((), (), s32[]{:S(2)}) async-start(), calls=%async_computation.5 | async-start | bytes 2359296 | tf_op jit(solution)/shard_map/reduce_scatter | solution.py:58
  68.7 3.5 copy-start.7
  79.6 101.7 %all-reduce.2.cloned.1.call-start = ((), (), s32[]{:S(2)}) async-start(), calls=%async_computation.6 | async-start | bytes 524288 | tf_op jit(solution)/shard_map/psum | solution.py:64
  147.8 105.7 %reduce-scatter.9.cloned.1.call-start = ((), (), s32[]{:S(2)}) async-start(), calls=%async_computation.7 | async-start | bytes 1179648 | tf_op jit(solution)/shard_map/reduce_scatter | solution.py:83
  185.3 3.9 copy-start.5
  189.1 138.4 %reduce-scatter.13.cloned.1.call-start = ((), (), s32[]{:S(2)}) async-start(), calls=%async_computation.10 | async-start | bytes 327680
  268.8 7.2 %copy-start.1 = (f32[32,4,128,128]{3,2,1,0:T(8,128)}, f32[32,4,128,128]{3,2,1,0:T(8,128)S(1)}, u32[]{:S(2)}) copy-start(f32[32,4,128,128]{3,2,1,0:T(8,128)S(1)} %multiply_add_fusion) | copy-start | bytes 25165828
  268.8 7.3 %copy-start.6 = (f32[128]{0:T(128)S(1)}, f32[128]{0:T(128)}, u32[]{:S(2)}) copy-start(f32[128]{0:T(128)} %param.30) | copy-start | bytes 1540
  268.8 38.3 %copy-start.3 = (bf16[512,512]{1,0:T(8,128)(2,1)S(1)}, bf16[512,512]{1,0:T(8,128)(2,1)}, u32[]{:S(2)}) copy-start(bf16[512,512]{1,0:T(8,128)(2,1)} %param.31) | copy-start | bytes 1572868
  276.0 109.9 %copy-start.4 = (f32[4096]{0:T(1024)S(1)}, f32[4096]{0:T(1024)}, u32[]{:S(2)}) copy-start(f32[4096]{0:T(1024)} %param.32) | copy-start | bytes 49156
  308.3 75.5 %all-gather.5.cloned.1.call-start = ((), (), s32[]{:S(2)}) async-start(), calls=%async_computation.8 | async-start | bytes 2162688 | tf_op jit(solution)/shard_map/all_gather | solution.py:13
  329.1 211.2 %reduce-scatter.11.cloned.1.call-start = ((), (), s32[]{:S(2)}) async-start(), calls=%async_computation.9 | async-start | bytes 4325376 | tf_op jit(solution)/shard_map/reduce_scatter | solution.py:23
  398.2 142.1 %copy-start.2 = (bf16[256,128]{1,0:T(8,128)(2,1)S(1)}, bf16[256,128]{1,0:T(8,128)(2,1)}, u32[]{:S(2)}) copy-start(bf16[256,128]{1,0:T(8,128)(2,1)} %add_convert_fusion.2) | copy-start | bytes 196612
Sparse Core Ops, SparseCore 0:
  10.8 55.6 all-gather.2
  79.7 67.9 reduce-scatter.6
  150.1 31.2 all-reduce.1
  189.2 64.1 reduce-scatter.8
  308.4 19.0 reduce-scatter.12
  330.8 52.9 all-gather.4
  398.4 141.8 reduce-scatter.10
where the time goes:
time: 550 us; the launch traced here: 549 us
  waiting for transfers between devices  418 us (76%)
  blocking collectives  52.4 us (10%)
  matrix products  36.1 us (7%)
  other arithmetic  20.7 us (4%)
  between operations  14.4 us (3%)
  local copies, waits for them, and re-layouts  6.21 us (1%)
    reduce_scatter x1, waiting for transfers between devices, down_sum(): lax.psum_scatter(jnp.dot(hidden, w_down, preferred_element_type=jnp.float...  142 us
    reduce_scatter x1, waiting for transfers between devices, per_device(): lax.psum_scatter(jnp.dot(hidden, pre_down, preferred_element_type=jnp.flo...  68.1 us
    all_gather x1, waiting for transfers between devices, per_device(): whole_rows = lax.all_gather(tokens, ('kv', 'tp'), axis=1, tiled=True)  58.6 us
    all_gather x1, waiting for transfers between devices, half_inputs(): lax.all_gather(activations, ('kv', 'tp'), axis=1, tiled=True)  54.4 us
    reduce_scatter x1, waiting for transfers between devices, per_device(): lax.psum_scatter(jnp.concatenate([jnp.dot(normed, weight_part, preferred_...  42.6 us
    psum x1, waiting for transfers between devices, per_device(): block_sum = lax.psum(kv_sums, 'tp').astype(jnp.float32)  32.8 us
    all_gather x1, blocking collectives, per_device(): lax.all_gather(mixed_in, 'kv', axis=0, tiled=True)  30.8 us
    psum x1, blocking collectives, per_device(): squares = lax.psum(jnp.sum(block_float * block_float, axis=1), 'kv')  21.6 us
  transfers between devices with their start and end apart: 7, of which 7 were waited for; matrix products, arithmetic and copies ran while one was open for 0% of the time, Pallas kernels for 0%

commit v1 on v0

--- a/solution.py
+++ b/solution.py
@@ -1,12 +1,324 @@
+import functools
+
 import jax
 import jax.numpy as jnp
 from jax import lax
+from jax.experimental import pallas as pl
+from jax.experimental.pallas import tpu as pltpu
 from jax.sharding import PartitionSpec as P
 
-D = 4096
-
-
 epsilon = 1e-06
+AXES = ("kv", "tp")
+LANES = 128
+CORE, NEAR_X, NEAR_Y, NEAR_Z = 1, 2, 4, 8
+WHOLE = pl.BlockSpec(memory_space=pltpu.VMEM)
+SCALAR = pl.BlockSpec(memory_space=pltpu.SMEM)
+float32, bfloat16 = jnp.float32, jnp.bfloat16
+
+
+def params(mib):
+    return pltpu.CompilerParams(vmem_limit_bytes=mib * 1024 * 1024)
+
+
+def device_count():
+    return lax.axis_size("kv") * lax.axis_size("tp")
+
+
+def flip(block, mask):
+    pairs = [(i, i ^ mask) for i in range(device_count())]
+    return lax.ppermute(block, AXES, pairs)
+
+
+def stack(blocks):
+    return jnp.stack(blocks)
+
+
+def gather_all(own):
+    z_count = device_count() // NEAR_Z
+    half = z_count // 2
+    column = stack([own] + [flip(own, NEAR_Z * z) for z in range(1, z_count)])
+    from_y = flip(column, NEAR_Y)
+    from_x = flip(column, NEAR_X)
+    core_own = flip(column, CORE)
+    diag_low = flip(from_y[:half], NEAR_X)
+    diag_high = flip(from_x[half:], NEAR_Y)
+    pieces = [
+        (0, 0, column),
+        (NEAR_Y, 0, from_y),
+        (NEAR_X, 0, from_x),
+        (NEAR_X | NEAR_Y, 0, diag_low),
+        (NEAR_X | NEAR_Y, half, diag_high),
+    ]
+    pieces += [(CORE, 0, core_own)] + [
+        (mask | CORE, first, flip(piece, CORE)) for mask, first, piece in pieces[1:]
+    ]
+    return pieces
+
+
+def half_body(masks, me_ref, gain_ref, gate_ref, up_ref, down_ref, *refs):
+    pieces, refs = refs[: len(masks)], refs[len(masks) :]
+    sends, keeps, (normed,) = refs[:4], refs[4:8], refs[8:]
+    me = me_ref[0]
+    rows, depth = normed.shape
+    width = LANES
+    squares = jnp.zeros((rows, width), float32)
+    for (mask, first), piece in zip(masks, pieces):
+
+        def place(z, total, mask=mask, first=first, piece=piece):
+            block = piece[z].astype(float32)
+            owner = me ^ (mask + NEAR_Z * (z + first))
+            columns = pl.ds(pl.multiple_of(owner * width, width), width)
+            normed[:, columns] = (block * gain_ref[:, columns]).astype(bfloat16)
+            return total + block * block
+
+        for z in range(piece.shape[0]):
+            squares = place(z, squares)
+    scale = lax.rsqrt(jnp.sum(squares, axis=1, keepdims=True) / depth + epsilon)
+    gate = scale * jnp.dot(normed[...], gate_ref[...], preferred_element_type=float32)
+    up = scale * jnp.dot(normed[...], up_ref[...], preferred_element_type=float32)
+    hidden = (gate * jax.nn.sigmoid(gate) * up).astype(bfloat16)
+    low = (me & CORE) == 0
+    for group, mask in enumerate((NEAR_X | NEAR_Y, NEAR_Y, NEAR_X, 0)):
+        for z in range(keeps[group].shape[0]):
+            pair = (me ^ (mask + NEAR_Z * z)) >> 1
+            columns = pl.ds(pl.multiple_of(pair * 2 * width, 2 * width), 2 * width)
+            both = jnp.dot(hidden, down_ref[:, columns], preferred_element_type=float32)
+            left, right = both[:, :width], both[:, width:]
+            keeps[group][z] = jnp.where(low, left, right)
+            sends[group][z] = jnp.where(low, right, left).astype(bfloat16)
+
+
+def half_partials(me, pieces, gain, gate, up, down):
+    depth = gain.shape[0]
+    z_count = device_count() // NEAR_Z
+    rows = pieces[0][2].shape[1]
+    masks = tuple((mask, first) for mask, first, _ in pieces)
+    group = (z_count, rows, LANES)
+    arrays = [piece for _, _, piece in pieces]
+    return pl.pallas_call(
+        functools.partial(half_body, masks),
+        out_shape=[jax.ShapeDtypeStruct(group, bfloat16)] * 4
+        + [jax.ShapeDtypeStruct(group, float32)] * 4,
+        in_specs=[SCALAR] + [WHOLE] * (4 + len(arrays)),
+        out_specs=[WHOLE] * 8,
+        scratch_shapes=[pltpu.VMEM((rows, depth), bfloat16)],
+        compiler_params=params(40),
+        name="half_step",
+    )(me, gain.reshape(1, depth), gate, up, down, *arrays)
+
+
+def scatter_sum(partials):
+    sends, keeps = partials[:4], partials[4:]
+    z_count = keeps[0].shape[0]
+    half = z_count // 2
+    received = [flip(block, CORE) for block in sends]
+    diag, to_y, to_x, own = [
+        keep + block.astype(float32) for keep, block in zip(keeps, received)
+    ]
+    diag = diag.astype(bfloat16)
+    low = flip(diag[:half], NEAR_X).astype(float32)
+    high = flip(diag[half:], NEAR_Y).astype(float32)
+    to_y = jnp.concatenate([to_y[:half] + low, to_y[half:]]).astype(bfloat16)
+    to_x = jnp.concatenate([to_x[:half], to_x[half:] + high]).astype(bfloat16)
+    own = own + flip(to_y, NEAR_Y).astype(float32) + flip(to_x, NEAR_X).astype(float32)
+    total = own[0]
+    for z in range(1, z_count):
+        total = total + flip(own[z].astype(bfloat16), NEAR_Z * z).astype(float32)
+    return total
+
+
+def project_body(me_ref, gain_ref, w0, w1, w2, w3, b0, b1, b2, b3, out_ref, normed, sums):
+    me = me_ref[0]
+    kv, tp = me // 4, me % 4
+    groups, own_rows, _ = out_ref.shape
+    rows, block = normed.shape
+    squares = jnp.zeros((rows, LANES), float32)
+    for mask, piece in enumerate((b0, b1, b2, b3)):
+        values = piece[...].astype(float32)
+        columns = pl.ds(pl.multiple_of((tp ^ mask) * LANES, LANES), LANES)
+        wide = pl.ds(pl.multiple_of((me ^ mask) * LANES, LANES), LANES)
+        normed[:, columns] = (values * gain_ref[:, wide]).astype(bfloat16)
+        squares = squares + values * values
+    total = jnp.sum(squares, axis=1, keepdims=True)
+    coarse = total.astype(bfloat16).astype(float32)
+    fine = total - coarse
+    lane = lax.broadcasted_iota(jnp.int32, (rows, LANES), 1)
+    sums[:, 4 * block :] = jnp.where(lane < LANES // 2, coarse, fine)
+    for index, weight in enumerate((w0, w1, w2, w3)):
+        sums[:, index * block : (index + 1) * block] = jnp.dot(
+            normed[...], weight[...], preferred_element_type=float32
+        )
+    for mask in range(groups):
+        start = pl.multiple_of((kv ^ mask) * own_rows, own_rows)
+        out_ref[mask] = sums[pl.ds(start, own_rows), :].astype(bfloat16)
+
+
+def project(me, blocks, mix_gain, weights, own_rows):
+    rows = blocks[0].shape[0]
+    block, width = weights[0].shape
+    groups = rows // own_rows
+    return pl.pallas_call(
+        project_body,
+        out_shape=jax.ShapeDtypeStruct((groups, own_rows, 4 * width + LANES), bfloat16),
+        in_specs=[SCALAR] + [WHOLE] * 9,
+        out_specs=WHOLE,
+        scratch_shapes=[
+            pltpu.VMEM((rows, block), bfloat16),
+            pltpu.VMEM((rows, 4 * width + LANES), float32),
+        ],
+        compiler_params=params(24),
+        name="project",
+    )(me, mix_gain.reshape(1, -1), *weights, *blocks)
+
+
+def scatter_rows(groups):
+    pairs = groups.reshape((-1, 2) + groups.shape[1:])
+    near = pairs[:, 0].astype(float32) + flip(pairs[:, 1], NEAR_Y).astype(float32)
+    total = near[0]
+    for z in range(1, near.shape[0]):
+        total = total + flip(near[z].astype(bfloat16), NEAR_Z * z).astype(float32)
+    return total
+
+
+def recur_body(steps, proj_ref, floor_ref, gain_ref, past_ref, new_ref, out_ref, readout):
+    step = pl.program_id(0)
+    rows, heads, size, _ = past_ref.shape
+    inner = heads * size
+    here = pl.ds(pl.multiple_of(step * rows, rows), rows)
+    floors = floor_ref[...]
+    pre_query = proj_ref[here, :inner]
+    pre_forget = proj_ref[here, inner : 2 * inner]
+    forget = floors + (1.0 - floors) * jax.nn.sigmoid(pre_forget)
+    written = (1.0 - floors) * jax.nn.sigmoid(-pre_forget)
+    query = pre_query * jax.nn.sigmoid(pre_query)
+    for h in range(heads):
+        lanes = slice(h * size, (h + 1) * size)
+        forget_t, written_t, query_t = (a[:, lanes].T for a in (forget, written, query))
+        value = proj_ref[here, 2 * inner + h * size : 2 * inner + (h + 1) * size]
+        reads = []
+        for n in range(rows):
+            column = slice(n, n + 1)
+            state = forget_t[:, column] * past_ref[n, h] + written_t[:, column] * value[column]
+            new_ref[n, h] = state
+            reads.append(jnp.sum(state * query_t[:, column], axis=0, keepdims=True))
+        readout[here, lanes] = jnp.concatenate(reads)
+
+    @pl.when(step == steps - 1)
+    def _():
+        gate = proj_ref[:, 3 * inner : 4 * inner]
+        gate = gate * jax.nn.sigmoid(gate)
+        for h in range(heads):
+            lanes = slice(h * size, (h + 1) * size)
+            part = readout[:, lanes]
+            power = jnp.mean(part * part, axis=1, keepdims=True)
+            part = part * lax.rsqrt(power + epsilon) * gain_ref[...]
+            out_ref[:, lanes] = (part * gate[:, lanes]).astype(bfloat16)
+
+
+def recur(projected, forget_floor, head_gain, past_state):
+    own_rows, heads, size, _ = past_state.shape
+    rows = 8 if own_rows % 8 == 0 else own_rows
+    steps = own_rows // rows
+    inner = heads * size
+    state = pl.BlockSpec((rows, heads, size, size), lambda i: (i, 0, 0, 0))
+    return pl.pallas_call(
+        functools.partial(recur_body, steps),
+        grid=(steps,),
+        out_shape=[
+            jax.ShapeDtypeStruct(past_state.shape, float32),
+            jax.ShapeDtypeStruct((own_rows, inner), bfloat16),
+        ],
+        in_specs=[
+            pl.BlockSpec(projected.shape, lambda i: (0, 0)),
+            pl.BlockSpec((1, inner), lambda i: (0, 0)),
+            pl.BlockSpec((1, size), lambda i: (0, 0)),
+            state,
+        ],
+        out_specs=[state, pl.BlockSpec((own_rows, inner), lambda i: (0, 0))],
+        scratch_shapes=[pltpu.VMEM((own_rows, inner), float32)],
+        compiler_params=params(24),
+        name="recur",
+    )(projected, forget_floor.reshape(1, inner), head_gain.reshape(1, size), past_state)
+
+
+def gather_rows(own):
+    z_count = lax.axis_size("kv") // 2
+    column = stack([own] + [flip(own, NEAR_Z * z) for z in range(1, z_count)])
+    return [column, flip(column, NEAR_Y)]
+
+
+def mix_body(me_ref, weight_ref, near, far, out_ref, rows_ref):
+    me = me_ref[0]
+    kv, tp = me // 4, me % 4
+    own_rows = near.shape[1]
+    for side, pieces in enumerate((near, far)):
+        for z in range(pieces.shape[0]):
+            start = pl.multiple_of((kv ^ (2 * z + side)) * own_rows, own_rows)
+            rows_ref[pl.ds(start, own_rows), :] = pieces[z]
+    for mask in range(out_ref.shape[0]):
+        columns = pl.ds(pl.multiple_of((tp ^ mask) * LANES, LANES), LANES)
+        out_ref[mask] = jnp.dot(
+            rows_ref[...], weight_ref[:, columns], preferred_element_type=float32
+        ).astype(bfloat16)
+
+
+def mix(me, pieces, weight):
+    count, own_rows, width = pieces[0].shape
+    rows = 2 * count * own_rows
+    blocks = weight.shape[1] // LANES
+    return pl.pallas_call(
+        mix_body,
+        out_shape=jax.ShapeDtypeStruct((blocks, rows, LANES), bfloat16),
+        in_specs=[SCALAR] + [WHOLE] * 3,
+        out_specs=WHOLE,
+        scratch_shapes=[pltpu.VMEM((rows, width), bfloat16)],
+        compiler_params=params(16),
+        name="mix",
+    )(me, weight, *pieces)
+
+
+def exchanged(
+    tokens,
+    past_state,
+    pre_gain,
+    pre_gate,
+    pre_up,
+    pre_down,
+    mix_gain,
+    query_weight,
+    forget_weight,
+    value_weight,
+    output_gate_weight,
+    forget_floor,
+    head_gain,
+    proj_out,
+    post_gain,
+    post_gate,
+    post_up,
+    post_down,
+):
+    me_scalar = lax.axis_index(AXES)
+    me = me_scalar.astype(jnp.int32).reshape(1)
+    depth = pre_gain.shape[0]
+    partials = half_partials(me, gather_all(tokens), pre_gain, pre_gate, pre_up, pre_down)
+    first = (tokens.astype(float32) + 0.5 * scatter_sum(partials)).astype(bfloat16)
+    from_x = flip(first, NEAR_X)
+    blocks = [first, flip(first, CORE), from_x, flip(from_x, CORE)]
+    weights = (query_weight, forget_weight, value_weight, output_gate_weight)
+    own_rows, heads, size, _ = past_state.shape
+    inner = heads * size
+    sums = scatter_rows(project(me, blocks, mix_gain, weights, own_rows))
+    squares = sums[:, 4 * inner] + sums[:, 4 * inner + LANES // 2]
+    projected = sums[:, : 4 * inner] * lax.rsqrt(squares / depth + epsilon)[:, None]
+    new_state, mixed_in = recur(projected, forget_floor, head_gain, past_state)
+    parts = mix(me, gather_rows(mixed_in), proj_out)
+    pairs = parts.reshape((2, 2) + parts.shape[1:])
+    near = pairs[:, 0].astype(float32) + flip(pairs[:, 1], CORE).astype(float32)
+    mixed = near[0] + flip(near[1].astype(bfloat16), NEAR_X).astype(float32)
+    second = (first.astype(float32) + mixed).astype(bfloat16)
+    partials = half_partials(me, gather_all(second), post_gain, post_gate, post_up, post_down)
+    result = (second.astype(float32) + 0.5 * scatter_sum(partials)).astype(bfloat16)
+    return (result, new_state)
 
 
 def half_inputs(activations, gain, w_gate, w_up):
@@ -15,7 +327,7 @@
     gate_acc = jnp.dot(normed, w_gate, preferred_element_type=jnp.float32)
     up_acc = jnp.dot(normed, w_up, preferred_element_type=jnp.float32)
     squares = jnp.sum(piece_float * piece_float, axis=1)
-    row_scale = lax.rsqrt(squares / D + epsilon)[:, None]
+    row_scale = lax.rsqrt(squares / piece_float.shape[1] + epsilon)[:, None]
     return (jax.nn.silu(row_scale * gate_acc) * (row_scale * up_acc)).astype(jnp.bfloat16)
 
 
@@ -93,7 +405,7 @@
         tiled=True,
     ).astype(jnp.float32)
     own_squares = lax.dynamic_slice_in_dim(squares, lax.axis_index("kv") * own_rows, own_rows, 0)
-    projected = projected * lax.rsqrt(own_squares / D + epsilon)[:, None]
+    projected = projected * lax.rsqrt(own_squares / pre_gain.shape[0] + epsilon)[:, None]
     pre_query, pre_forget, pre_value, pre_gate_out = jnp.split(projected, 4, axis=1)
     local_heads = past_state.shape[1]
     head_width = past_state.shape[2]
@@ -153,8 +465,14 @@
         P(None, ("kv", "tp")),
         P(("kv", "tp"), None),
     )
+    def local(*arrays):
+        width = arrays[0].shape[1]
+        fits = mesh.shape["tp"] == 4 and mesh.shape["kv"] in (4, 8, 16)
+        plan = exchanged if fits and width == LANES else per_device
+        return plan(*arrays)
+
     return jax.shard_map(
-        per_device,
+        local,
         mesh=mesh,
         in_specs=placed,
         out_specs=(P(None, ("kv", "tp")), P("kv", "tp", None, None)),

time: 550 us -> 208 us (0.38)
  waiting for transfers between devices: 418 us -> 101 us
  blocking collectives: 52.4 us -> 0 us
  starting transfers between devices: 0.5 us -> 51.7 us
  matrix products: 36.1 us -> 0 us
  Pallas kernels: 0 us -> 22.3 us
  local copies, waits for them, and re-layouts: 6.21 us -> 27.5 us
  other arithmetic: 20.7 us -> 3.01 us
  between operations: 14.4 us -> 1.2 us
    reduce_scatter x3 -> x0, waiting for transfers between devices: 253 us -> none  [the longest x1 142 us: down_sum(): lax.psum_scatter(jnp.dot(hidden, w_down, preferred_element_type=jnp.float...]
    all_gather x2 -> x0, waiting for transfers between devices: 113 us -> none  [the longest x1 58.6 us: per_device(): whole_rows = lax.all_gather(tokens, ('kv', 'tp'), axis=1, tiled=True)]
    ppermute x0 -> x59, waiting for transfers between devices: none -> 101 us  [flip(): return lax.ppermute(block, AXES, pairs)]
    ppermute x0 -> x59, starting transfers between devices: none -> 51.7 us  [flip(): return lax.ppermute(block, AXES, pairs)]
    dot_general x10 -> x0, matrix products: 36.1 us -> none  [the longest x1 8.94 us: down_sum(): jnp.dot(hidden, w_down, preferred_element_type=jnp.float32)]
    psum x1 -> x0, waiting for transfers between devices: 32.8 us -> none  [per_device(): block_sum = lax.psum(kv_sums, 'tp').astype(jnp.float32)]
    all_gather x1 -> x0, blocking collectives: 30.8 us -> none  [per_device(): lax.all_gather(mixed_in, 'kv', axis=0, tiled=True)]
    pallas_call x0 -> x5, Pallas kernels: none -> 22.3 us  [the longest x2 11.4 us: half_partials(): pl.pallas_call(functools.partial(half_body, masks), out_shape=[jax.ShapeD...]
  transfers between devices with their start and end apart: 7 -> 59, of which waited for: 7 -> 38; matrix products, arithmetic and copies ran while one was open for 0% -> 10% of each run, Pallas kernels for 0% -> 0%
where the time goes in v1:
time: 208 us; the launch traced here: 207 us
  waiting for transfers between devices  101 us (49%)
  starting transfers between devices  51.7 us (25%)
  local copies, waits for them, and re-layouts  27.5 us (13%)
  Pallas kernels  22.3 us (11%)
  other arithmetic  3.01 us (1%)
    ppermute x59, waiting for transfers between devices, flip(): return lax.ppermute(block, AXES, pairs)  101 us
    ppermute x59, starting transfers between devices, flip(): return lax.ppermute(block, AXES, pairs)  51.7 us
    unnamed x42, local copies, waits for them, and re-layouts  23.6 us
    pallas_call x2, Pallas kernels, half_partials(): pl.pallas_call(functools.partial(half_body, masks), out_shape=[jax.ShapeD...  11.4 us
    pallas_call x1, Pallas kernels, recur(): pl.pallas_call(functools.partial(recur_body, steps), grid=(steps,), out_s...  9.59 us
  transfers between devices with their start and end apart: 59, of which 38 were waited for; matrix products, arithmetic and copies ran while one was open for 10% of the time, Pallas kernels for 0%

profile of v1, /device:TPU:0, one launch (start us, length us, event | category | flops | bytes accessed | tf_op | source)
XLA Modules:
  0.0 206.8 jit_solution(11288153203891101306)
XLA Ops:
  0.6 3.1 %collective-permute-start = (bf16[256,128]{1,0:T(8,128)(2,1)}, bf16[256,128]{1,0:T(8,128)(2,1)S(1)}, u32[]{:S(2)}, u32[]{:S(2)}) collective-permute-start(bf16[256,128]{1,0:T(8,128)(2,1)} %param.18), channel_id=1, source_target_pairs={{0,8},{1,9},{2,10},{3,11},{4,12},{5,13},{6,14},{7,15},{8,0},{9,1},... | collective-permute-start | bytes 196616 | tf_op jit(solution)/shard_map/ppermute | solution.py:29
  6.3 4.5 %collective-permute-done.2 = bf16[256,128]{1,0:T(8,128)(2,1)S(1)} collective-permute-done((bf16[256,128]{1,0:T(8,128)(2,1)}, bf16[256,128]{1,0:T(8,128)(2,1)S(1)}, u32[]{:S(2)}, u32[]{:S(2)}) %collective-permute-start.2) | collective-permute-done | bytes 65568 | tf_op jit(solution)/shard_map/ppermute | solution.py:29
  16.9 5.3 %collective-permute-done.4.refs_2_ = bf16[4,256,128]{2,1,0:T(8,128)(2,1)} collective-permute-done((bf16[4,256,128]{2,1,0:T(8,128)(2,1)S(1)}, bf16[4,256,128]{2,1,0:T(8,128)(2,1)}, u32[]{:S(2)}, u32[]{:S(2)}) %collective-permute-start.4) | collective-permute-done | bytes 262176 | tf_op jit(solution)/shard_map/ppermute | solution.py:29
  28.1 3.6 %collective-permute-done.5.refs_3_ = bf16[2,256,128]{2,1,0:T(8,128)(2,1)} collective-permute-done((bf16[2,256,128]{2,1,0:T(8,128)(2,1)S(1)}, bf16[2,256,128]{2,1,0:T(8,128)(2,1)}, u32[]{:S(2)}, u32[]{:S(2)}) %collective-permute-start.5) | collective-permute-done | bytes 131104 | tf_op jit(solution)/shard_map/ppermute | solution.py:29
  31.7 3.4 %copy.24.gate_ref = bf16[4096,352]{1,0:T(8,128)(2,1)S(1)} copy(bf16[4096,352]{0,1:T(8,128)(2,1)} %param.21) | data formatting | bytes 5767168 | tf_op args[3]
  35.1 4.6 %copy.25.up_ref = bf16[4096,352]{1,0:T(8,128)(2,1)} copy(bf16[4096,352]{0,1:T(8,128)(2,1)} %param.22) | data formatting | bytes 5767168 | tf_op args[4]
  43.4 5.7 %half_step.2 = (bf16[4,256,128]{2,1,0:T(8,128)(2,1)S(1)}, bf16[4,256,128]{2,1,0:T(8,128)(2,1)S(1)}, bf16[4,256,128]{2,1,0:T(8,128)(2,1)S(1)}, bf16[4,256,128]{2,...) custom-call(s32[1]{0:T(128)} %bitcast.me_ref, ...), custom_call_target="tpu_custom_call" | custom-call | tf_op jit(solution)/shard_map/half_step/pallas_call | solution.py:98
  53.5 3.6 %collective-permute-done.15 = bf16[2,256,128]{2,1,0:T(8,128)(2,1)S(1)} collective-permute-done((bf16[2,256,128]{2,1,0:T(8,128)(2,1)S(1)}, bf16[2,256,128]{2,1,0:T(8,128)(2,1)S(1)}, u32[]{:S(2)}, u32[]{:S(2)}) %collective-permute-start.15) | collective-permute-done | bytes 131104 | tf_op jit(solution)/shard_map/ppermute | solution.py:29
  59.4 5.6 %collective-permute-done.16 = bf16[4,256,128]{2,1,0:T(8,128)(2,1)S(1)} collective-permute-done((bf16[4,256,128]{2,1,0:T(8,128)(2,1)S(1)}, bf16[4,256,128]{2,1,0:T(8,128)(2,1)S(1)}, u32[]{:S(2)}, u32[]{:S(2)}) %collective-permute-start.16) | collective-permute-done | bytes 262176 | tf_op jit(solution)/shard_map/ppermute | solution.py:29
  75.1 3.4 %collective-permute-done.24.b2 = bf16[256,128]{1,0:T(8,128)(2,1)S(1)} collective-permute-done((bf16[256,128]{1,0:T(8,128)(2,1)S(1)}, bf16[256,128]{1,0:T(8,128)(2,1)S(1)}, u32[]{:S(2)}, u32[]{:S(2)}) %collective-permute-start.24) | collective-permute-done | bytes 65568 | tf_op jit(solution)/shard_map/ppermute | solution.py:29
  81.7 13.7 %collective-permute-done.26 = bf16[4,32,2176]{2,1,0:T(8,128)(2,1)S(1)} collective-permute-done((bf16[4,32,2176]{2,1,0:T(8,128)(2,1)S(1)}, bf16[4,32,2176]{2,1,0:T(8,128)(2,1)S(1)}, u32[]{:S(2)}, u32[]{:S(2)}) %collective-permute-start.26) | collective-permute-done | bytes 557088 | tf_op jit(solution)/shard_map/ppermute | solution.py:29
  99.2 3.2 %collective-permute-done.27 = bf16[32,2176]{1,0:T(8,128)(2,1)S(1)} collective-permute-done((bf16[32,2176]{1,0:T(8,128)(2,1)S(1)}, bf16[32,2176]{1,0:T(8,128)(2,1)S(1)}, u32[]{:S(2)}, u32[]{:S(2)}) %collective-permute-start.27) | collective-permute-done | bytes 139296 | tf_op jit(solution)/shard_map/ppermute | solution.py:29
  102.4 3.0 %collective-permute-done.29 = bf16[32,2176]{1,0:T(8,128)(2,1)S(1)} collective-permute-done((bf16[32,2176]{1,0:T(8,128)(2,1)S(1)}, bf16[32,2176]{1,0:T(8,128)(2,1)S(1)}, u32[]{:S(2)}, u32[]{:S(2)}) %collective-permute-start.29) | collective-permute-done | bytes 139296 | tf_op jit(solution)/shard_map/ppermute | solution.py:29
  105.4 5.3 %collective-permute-done.28 = bf16[32,2176]{1,0:T(8,128)(2,1)S(1)} collective-permute-done((bf16[32,2176]{1,0:T(8,128)(2,1)S(1)}, bf16[32,2176]{1,0:T(8,128)(2,1)S(1)}, u32[]{:S(2)}, u32[]{:S(2)}) %collective-permute-start.28) | collective-permute-done | bytes 139296 | tf_op jit(solution)/shard_map/ppermute | solution.py:29
  111.1 9.6 %recur.1 = (f32[32,4,128,128]{3,2,1,0:T(8,128)}, bf16[32,512]{1,0:T(8,128)(2,1)S(1)}) custom-call(f32[32,2048]{1,0:T(8,128)S(1)} %slice_multiply_fusion.proj_ref, f32[1,512]{1,0:T(1,128)S(1)} %bitcast.118, f32[1,128]{1,0:T(1,128)S(1)} %bitcast.119, f32[32,4,128,128]{3,2,1,0:T(8,128)S(1)} %bitcast.109), custom_call_target="tpu_custom_call" | custom-call | tf_op jit(solution)/shard_map/recur/pallas_call | solution.py:224
  128.5 4.0 %collective-permute-done.33.far = bf16[4,32,512]{2,1,0:T(8,128)(2,1)S(1)} collective-permute-done((bf16[4,32,512]{2,1,0:T(8,128)(2,1)S(1)}, bf16[4,32,512]{2,1,0:T(8,128)(2,1)S(1)}, u32[]{:S(2)}, u32[]{:S(2)}) %collective-permute-start.33) | collective-permute-done | bytes 131104 | tf_op jit(solution)/shard_map/ppermute | solution.py:29
  135.4 3.3 %collective-permute-done.35 = bf16[256,128]{1,0:T(8,128)(2,1)S(1)} collective-permute-done((bf16[256,128]{1,0:T(8,128)(2,1)S(1)}, bf16[256,128]{1,0:T(8,128)(2,1)S(1)}, u32[]{:S(2)}, u32[]{:S(2)}) %collective-permute-start.35) | collective-permute-done | bytes 65568 | tf_op jit(solution)/shard_map/ppermute | solution.py:29
  149.8 4.2 %collective-permute-done.40.refs_2_ = bf16[4,256,128]{2,1,0:T(8,128)(2,1)} collective-permute-done((bf16[4,256,128]{2,1,0:T(8,128)(2,1)S(1)}, bf16[4,256,128]{2,1,0:T(8,128)(2,1)}, u32[]{:S(2)}, u32[]{:S(2)}) %collective-permute-start.40) | collective-permute-done | bytes 262176 | tf_op jit(solution)/shard_map/ppermute | solution.py:29
  159.9 3.1 %collective-permute-done.41.refs_3_ = bf16[2,256,128]{2,1,0:T(8,128)(2,1)} collective-permute-done((bf16[2,256,128]{2,1,0:T(8,128)(2,1)S(1)}, bf16[2,256,128]{2,1,0:T(8,128)(2,1)}, u32[]{:S(2)}, u32[]{:S(2)}) %collective-permute-start.41) | collective-permute-done | bytes 131104 | tf_op jit(solution)/shard_map/ppermute | solution.py:29
  163.0 3.4 %copy.30.gate_ref = bf16[4096,352]{1,0:T(8,128)(2,1)S(1)} copy(bf16[4096,352]{0,1:T(8,128)(2,1)} %param.33) | data formatting | bytes 5767168 | tf_op args[15]
  166.4 4.8 %copy.31.up_ref = bf16[4096,352]{1,0:T(8,128)(2,1)} copy(bf16[4096,352]{0,1:T(8,128)(2,1)} %param.34) | data formatting | bytes 5767168 | tf_op args[16]
  174.9 5.7 %half_step.3 = (bf16[4,256,128]{2,1,0:T(8,128)(2,1)S(1)}, bf16[4,256,128]{2,1,0:T(8,128)(2,1)S(1)}, bf16[4,256,128]{2,1,0:T(8,128)(2,1)S(1)}, bf16[4,256,128]{2,...) custom-call(s32[1]{0:T(128)} %bitcast.me_ref, ...), custom_call_target="tpu_custom_call" | custom-call | tf_op jit(solution)/shard_map/half_step/pallas_call | solution.py:98
  185.0 3.7 %collective-permute-done.51 = bf16[2,256,128]{2,1,0:T(8,128)(2,1)S(1)} collective-permute-done((bf16[2,256,128]{2,1,0:T(8,128)(2,1)S(1)}, bf16[2,256,128]{2,1,0:T(8,128)(2,1)S(1)}, u32[]{:S(2)}, u32[]{:S(2)}) %collective-permute-start.51) | collective-permute-done | bytes 131104 | tf_op jit(solution)/shard_map/ppermute | solution.py:29
  191.0 5.6 %collective-permute-done.52 = bf16[4,256,128]{2,1,0:T(8,128)(2,1)S(1)} collective-permute-done((bf16[4,256,128]{2,1,0:T(8,128)(2,1)S(1)}, bf16[4,256,128]{2,1,0:T(8,128)(2,1)S(1)}, u32[]{:S(2)}, u32[]{:S(2)}) %collective-permute-start.52) | collective-permute-done | bytes 262176 | tf_op jit(solution)/shard_map/ppermute | solution.py:29
  (185 shorter events, 90.3 us)
Async XLA Ops:
  3.7 7.1 %collective-permute-start.2 = (bf16[256,128]{1,0:T(8,128)(2,1)}, bf16[256,128]{1,0:T(8,128)(2,1)S(1)}, u32[]{:S(2)}, u32[]{:S(2)}) collective-permute-start(bf16[256,128]{1,0:T(8,128)(2,1)} %param.18), channel_id=1, source_target_pairs={{0,24},{1,25},{2,26},{3,27},{4,28},{5,29},{6,30},{7,31},{8,16},{9,... | collective-permute-start | bytes 196616 | tf_op jit(solution)/shard_map/ppermute | solution.py:29
  13.8 8.3 %collective-permute-start.4 = (bf16[4,256,128]{2,1,0:T(8,128)(2,1)S(1)}, bf16[4,256,128]{2,1,0:T(8,128)(2,1)}, u32[]{:S(2)}, u32[]{:S(2)}) collective-permute-start(bf16[4,256,128]{2,1,0:T(8,128)(2,1)S(1)} %pad_maximum_fusion.refs_0_), channel_id=1, source_target_pairs={{0,2},{1,3},{2,0},{3,1},{4,6},{5,7},{6,4},{7,5},{8,10},{9,11},{10,... | collective-permute-start | bytes 786440 | tf_op jit(solution)/shard_map/ppermute | solution.py:29
  15.3 9.3 %collective-permute-start.3 = (bf16[4,256,128]{2,1,0:T(8,128)(2,1)S(1)}, bf16[4,256,128]{2,1,0:T(8,128)(2,1)}, u32[]{:S(2)}, u32[]{:S(2)}) collective-permute-start(bf16[4,256,128]{2,1,0:T(8,128)(2,1)S(1)} %pad_maximum_fusion.refs_0_), channel_id=1, source_target_pairs={{0,4},{1,5},{2,6},{3,7},{4,0},{5,1},{6,2},{7,3},{8,12},{9,13},{10,... | collective-permute-start | bytes 786440 | tf_op jit(solution)/shard_map/ppermute | solution.py:29
  16.8 22.8 %collective-permute-start.7 = (bf16[4,256,128]{2,1,0:T(8,128)(2,1)S(1)}, bf16[4,256,128]{2,1,0:T(8,128)(2,1)}, u32[]{:S(2)}, u32[]{:S(2)}) collective-permute-start(bf16[4,256,128]{2,1,0:T(8,128)(2,1)S(1)} %pad_maximum_fusion.refs_0_), channel_id=1, source_target_pairs={{0,1},{1,0},{2,3},{3,2},{4,5},{5,4},{6,7},{7,6},{8,9},{9,8},{10,11... | collective-permute-start | bytes 786440 | tf_op jit(solution)/shard_map/ppermute | solution.py:29
  24.6 15.1 %collective-permute-start.9 = (bf16[4,256,128]{2,1,0:T(8,128)(2,1)}, bf16[4,256,128]{2,1,0:T(8,128)(2,1)}, u32[]{:S(2)}, u32[]{:S(2)}) collective-permute-start(bf16[4,256,128]{2,1,0:T(8,128)(2,1)} %collective-permute-done.4.refs_2_), channel_id=1, source_target_pairs={{0,1},{1,0},{2,3},{3,2},{4,5},{5,4},{6,7},{7,6},{8,9},{9,8},{10,11... | collective-permute-start | bytes 786440 | tf_op jit(solution)/shard_map/ppermute | solution.py:29
  25.5 14.1 %collective-permute-start.8 = (bf16[4,256,128]{2,1,0:T(8,128)(2,1)}, bf16[4,256,128]{2,1,0:T(8,128)(2,1)}, u32[]{:S(2)}, u32[]{:S(2)}) collective-permute-start(bf16[4,256,128]{2,1,0:T(8,128)(2,1)} %collective-permute-done.3.refs_1_), channel_id=1, source_target_pairs={{0,1},{1,0},{2,3},{3,2},{4,5},{5,4},{6,7},{7,6},{8,9},{9,8},{10,11... | collective-permute-start | bytes 786440 | tf_op jit(solution)/shard_map/ppermute | solution.py:29
  28.1 11.6 %collective-permute-start.11 = (bf16[2,256,128]{2,1,0:T(8,128)(2,1)S(1)}, bf16[2,256,128]{2,1,0:T(8,128)(2,1)}, u32[]{:S(2)}, u32[]{:S(2)}) collective-permute-start(bf16[2,256,128]{2,1,0:T(8,128)(2,1)S(1)} %collective-permute-done.6.refs_4_), channel_id=1, source_target_pairs={{0,1},{1,0},{2,3},{3,2},{4,5},{5,4},{6,7},{7,6},{8,9},{9,8},{10,11... | collective-permute-start | bytes 393224 | tf_op jit(solution)/shard_map/ppermute | solution.py:29
  31.7 8.0 %collective-permute-start.10 = (bf16[2,256,128]{2,1,0:T(8,128)(2,1)}, bf16[2,256,128]{2,1,0:T(8,128)(2,1)}, u32[]{:S(2)}, u32[]{:S(2)}) collective-permute-start(bf16[2,256,128]{2,1,0:T(8,128)(2,1)} %collective-permute-done.5.refs_3_), channel_id=1, source_target_pairs={{0,1},{1,0},{2,3},{3,2},{4,5},{5,4},{6,7},{7,6},{8,9},{9,8},{10,11... | collective-permute-start | bytes 393224 | tf_op jit(solution)/shard_map/ppermute | solution.py:29
  49.8 9.7 %collective-permute-start.12 = (bf16[4,256,128]{2,1,0:T(8,128)(2,1)S(1)}, bf16[4,256,128]{2,1,0:T(8,128)(2,1)S(1)}, u32[]{:S(2)}, u32[]{:S(2)}) collective-permute-start(bf16[4,256,128]{2,1,0:T(8,128)(2,1)S(1)} %get-tuple-element.21), channel_id=1, source_target_pairs={{0,1},{1,0},{2,3},{3,2},{4,5},{5,4},{6,7},{7,6},{8,9},{9,8},{10,11... | collective-permute-start | bytes 786440 | tf_op jit(solution)/shard_map/ppermute | solution.py:29
  57.2 7.8 %collective-permute-start.16 = (bf16[4,256,128]{2,1,0:T(8,128)(2,1)S(1)}, bf16[4,256,128]{2,1,0:T(8,128)(2,1)S(1)}, u32[]{:S(2)}, u32[]{:S(2)}) collective-permute-start(bf16[4,256,128]{2,1,0:T(8,128)(2,1)S(1)} %pad_maximum_fusion.1), channel_id=1, source_target_pairs={{0,4},{1,5},{2,6},{3,7},{4,0},{5,1},{6,2},{7,3},{8,12},{9,13},{10,... | collective-permute-start | bytes 786440 | tf_op jit(solution)/shard_map/ppermute | solution.py:29
  58.5 7.5 %collective-permute-start.19 = (bf16[4,256,128]{2,1,0:T(8,128)(2,1)S(1)}, bf16[4,256,128]{2,1,0:T(8,128)(2,1)S(1)}, u32[]{:S(2)}, u32[]{:S(2)}) collective-permute-start(bf16[4,256,128]{2,1,0:T(8,128)(2,1)S(1)} %pad_maximum_fusion.2), channel_id=1, source_target_pairs={{0,2},{1,3},{2,0},{3,1},{4,6},{5,7},{6,4},{7,5},{8,10},{9,11},{10,... | collective-permute-start | bytes 786440 | tf_op jit(solution)/shard_map/ppermute | solution.py:29
  80.7 14.7 %collective-permute-start.26 = (bf16[4,32,2176]{2,1,0:T(8,128)(2,1)S(1)}, bf16[4,32,2176]{2,1,0:T(8,128)(2,1)S(1)}, u32[]{:S(2)}, u32[]{:S(2)}) collective-permute-start(bf16[4,32,2176]{2,1,0:T(8,128)(2,1)S(1)} %slice_bitcast_fusion), channel_id=1, source_target_pairs={{0,4},{1,5},{2,6},{3,7},{4,0},{5,1},{6,2},{7,3},{8,12},{9,13},{10,... | collective-permute-start | bytes 1671176 | tf_op jit(solution)/shard_map/ppermute | solution.py:29
  95.7 9.7 %collective-permute-start.29 = (bf16[32,2176]{1,0:T(8,128)(2,1)S(1)}, bf16[32,2176]{1,0:T(8,128)(2,1)S(1)}, u32[]{:S(2)}, u32[]{:S(2)}) collective-permute-start(bf16[32,2176]{1,0:T(8,128)(2,1)S(1)} %get-tuple-element.45), channel_id=1, source_target_pairs={{0,24},{1,25},{2,26},{3,27},{4,28},{5,29},{6,30},{7,31},{8,16},{9,... | collective-permute-start | bytes 417800 | tf_op jit(solution)/shard_map/ppermute | solution.py:29
  98.1 12.6 %collective-permute-start.28 = (bf16[32,2176]{1,0:T(8,128)(2,1)S(1)}, bf16[32,2176]{1,0:T(8,128)(2,1)S(1)}, u32[]{:S(2)}, u32[]{:S(2)}) collective-permute-start(bf16[32,2176]{1,0:T(8,128)(2,1)S(1)} %get-tuple-element.46), channel_id=1, source_target_pairs={{0,16},{1,17},{2,18},{3,19},{4,20},{5,21},{6,22},{7,23},{8,24},{9,... | collective-permute-start | bytes 417800 | tf_op jit(solution)/shard_map/ppermute | solution.py:29
  138.8 6.9 %collective-permute-start.38 = (bf16[256,128]{1,0:T(8,128)(2,1)S(1)}, bf16[256,128]{1,0:T(8,128)(2,1)S(1)}, u32[]{:S(2)}, u32[]{:S(2)}) collective-permute-start(bf16[256,128]{1,0:T(8,128)(2,1)S(1)} %fusion.15), channel_id=1, source_target_pairs={{0,24},{1,25},{2,26},{3,27},{4,28},{5,29},{6,30},{7,31},{8,16},{9,... | collective-permute-start | bytes 196616 | tf_op jit(solution)/shard_map/ppermute | solution.py:29
  148.2 7.7 %collective-permute-start.39 = (bf16[4,256,128]{2,1,0:T(8,128)(2,1)S(1)}, bf16[4,256,128]{2,1,0:T(8,128)(2,1)}, u32[]{:S(2)}, u32[]{:S(2)}) collective-permute-start(bf16[4,256,128]{2,1,0:T(8,128)(2,1)S(1)} %pad_maximum_fusion.3.refs_0_), channel_id=1, source_target_pairs={{0,4},{1,5},{2,6},{3,7},{4,0},{5,1},{6,2},{7,3},{8,12},{9,13},{10,... | collective-permute-start | bytes 786440 | tf_op jit(solution)/shard_map/ppermute | solution.py:29
  149.7 21.4 %collective-permute-start.43 = (bf16[4,256,128]{2,1,0:T(8,128)(2,1)S(1)}, bf16[4,256,128]{2,1,0:T(8,128)(2,1)}, u32[]{:S(2)}, u32[]{:S(2)}) collective-permute-start(bf16[4,256,128]{2,1,0:T(8,128)(2,1)S(1)} %pad_maximum_fusion.3.refs_0_), channel_id=1, source_target_pairs={{0,1},{1,0},{2,3},{3,2},{4,5},{5,4},{6,7},{7,6},{8,9},{9,8},{10,11... | collective-permute-start | bytes 786440 | tf_op jit(solution)/shard_map/ppermute | solution.py:29
  155.9 15.3 %collective-permute-start.45 = (bf16[4,256,128]{2,1,0:T(8,128)(2,1)}, bf16[4,256,128]{2,1,0:T(8,128)(2,1)}, u32[]{:S(2)}, u32[]{:S(2)}) collective-permute-start(bf16[4,256,128]{2,1,0:T(8,128)(2,1)} %collective-permute-done.40.refs_2_), channel_id=1, source_target_pairs={{0,1},{1,0},{2,3},{3,2},{4,5},{5,4},{6,7},{7,6},{8,9},{9,8},{10,11... | collective-permute-start | bytes 786440 | tf_op jit(solution)/shard_map/ppermute | solution.py:29
  156.8 14.4 %collective-permute-start.44 = (bf16[4,256,128]{2,1,0:T(8,128)(2,1)}, bf16[4,256,128]{2,1,0:T(8,128)(2,1)}, u32[]{:S(2)}, u32[]{:S(2)}) collective-permute-start(bf16[4,256,128]{2,1,0:T(8,128)(2,1)} %collective-permute-done.39.refs_1_), channel_id=1, source_target_pairs={{0,1},{1,0},{2,3},{3,2},{4,5},{5,4},{6,7},{7,6},{8,9},{9,8},{10,11... | collective-permute-start | bytes 786440 | tf_op jit(solution)/shard_map/ppermute | solution.py:29
  159.9 11.3 %collective-permute-start.47 = (bf16[2,256,128]{2,1,0:T(8,128)(2,1)S(1)}, bf16[2,256,128]{2,1,0:T(8,128)(2,1)}, u32[]{:S(2)}, u32[]{:S(2)}) collective-permute-start(bf16[2,256,128]{2,1,0:T(8,128)(2,1)S(1)} %collective-permute-done.42.refs_4_), channel_id=1, source_target_pairs={{0,1},{1,0},{2,3},{3,2},{4,5},{5,4},{6,7},{7,6},{8,9},{9,8},{10,11... | collective-permute-start | bytes 393224 | tf_op jit(solution)/shard_map/ppermute | solution.py:29
  163.0 8.2 %collective-permute-start.46 = (bf16[2,256,128]{2,1,0:T(8,128)(2,1)}, bf16[2,256,128]{2,1,0:T(8,128)(2,1)}, u32[]{:S(2)}, u32[]{:S(2)}) collective-permute-start(bf16[2,256,128]{2,1,0:T(8,128)(2,1)} %collective-permute-done.41.refs_3_), channel_id=1, source_target_pairs={{0,1},{1,0},{2,3},{3,2},{4,5},{5,4},{6,7},{7,6},{8,9},{9,8},{10,11... | collective-permute-start | bytes 393224 | tf_op jit(solution)/shard_map/ppermute | solution.py:29
  181.3 9.7 %collective-permute-start.48 = (bf16[4,256,128]{2,1,0:T(8,128)(2,1)S(1)}, bf16[4,256,128]{2,1,0:T(8,128)(2,1)S(1)}, u32[]{:S(2)}, u32[]{:S(2)}) collective-permute-start(bf16[4,256,128]{2,1,0:T(8,128)(2,1)S(1)} %get-tuple-element.30), channel_id=1, source_target_pairs={{0,1},{1,0},{2,3},{3,2},{4,5},{5,4},{6,7},{7,6},{8,9},{9,8},{10,11... | collective-permute-start | bytes 786440 | tf_op jit(solution)/shard_map/ppermute | solution.py:29
  188.8 7.8 %collective-permute-start.52 = (bf16[4,256,128]{2,1,0:T(8,128)(2,1)S(1)}, bf16[4,256,128]{2,1,0:T(8,128)(2,1)S(1)}, u32[]{:S(2)}, u32[]{:S(2)}) collective-permute-start(bf16[4,256,128]{2,1,0:T(8,128)(2,1)S(1)} %pad_maximum_fusion.4), channel_id=1, source_target_pairs={{0,4},{1,5},{2,6},{3,7},{4,0},{5,1},{6,2},{7,3},{8,12},{9,13},{10,... | collective-permute-start | bytes 786440 | tf_op jit(solution)/shard_map/ppermute | solution.py:29
  190.0 7.5 %collective-permute-start.55 = (bf16[4,256,128]{2,1,0:T(8,128)(2,1)S(1)}, bf16[4,256,128]{2,1,0:T(8,128)(2,1)S(1)}, u32[]{:S(2)}, u32[]{:S(2)}) collective-permute-start(bf16[4,256,128]{2,1,0:T(8,128)(2,1)S(1)} %pad_maximum_fusion.5), channel_id=1, source_target_pairs={{0,2},{1,3},{2,0},{3,1},{4,6},{5,7},{6,4},{7,5},{8,10},{9,11},{10,... | collective-permute-start | bytes 786440 | tf_op jit(solution)/shard_map/ppermute | solution.py:29
  (54 other events, 548.7 us)

commit v2 on v1

v2 whole, which is shorter than its diff:
```python
import functools

import jax
import jax.numpy as jnp
from jax import lax
from jax.experimental import pallas as pl
from jax.experimental.pallas import tpu as pltpu
from jax.sharding import PartitionSpec as P


epsilon = 1e-06
AXES = ("kv", "tp")
LANES = 128
CORE, NEAR_X, NEAR_Y, NEAR_Z = 1, 2, 4, 8
WHOLE = pl.BlockSpec(memory_space=pltpu.VMEM)
SCALAR = pl.BlockSpec(memory_space=pltpu.SMEM)
float32, bfloat16 = jnp.float32, jnp.bfloat16


def params(mib):
    return pltpu.CompilerParams(vmem_limit_bytes=mib * 1024 * 1024)


def device_count():
    return lax.axis_size("kv") * lax.axis_size("tp")


def flip(block, mask):
    pairs = [(i, i ^ mask) for i in range(device_count())]
    return lax.ppermute(block, AXES, pairs)


def stack(blocks):
    return jnp.stack(blocks)


def visit_body(first_ref, *refs):
    refs[-1][...] = first_ref[: refs[-1].shape[0], : refs[-1].shape[1]].astype(float32)


def visit(*arrays):
    return pl.pallas_call(
        visit_body,
        out_shape=jax.ShapeDtypeStruct((16, LANES), float32),
        in_specs=[WHOLE] * len(arrays),
        out_specs=WHOLE,
        compiler_params=params(16),
        name="visit",
    )(*arrays)


def stripes(block, axis, count):
    return jnp.split(block, count, axis=axis)


def gather_all(own, count=1):
    z_count = device_count() // NEAR_Z
    owns = stripes(own, 0, count)
    columns = [[part] + [flip(part, NEAR_Z * z) for z in range(1, z_count)] for part in owns]
    columns = [stack(column) for column in columns]
    pieces = []
    for index, column in enumerate(columns):
        row = index * column.shape[1]
        near = [(0, row, column)]
        for mask in (NEAR_X | NEAR_Y, NEAR_Y, NEAR_X):
            near.append((mask, row, flip(column, mask)))
        pieces += near
        pieces += [(mask | CORE, row, flip(piece, CORE)) for mask, row, piece in near]
    return pieces


def half_body(masks, me_ref, gain_ref, gate_ref, up_ref, down_ref, *refs):
    pieces, refs = refs[: len(masks)], refs[-9:]
    sends, keeps, (normed,) = refs[:4], refs[4:8], refs[8:]
    me = me_ref[0]
    _, depth = normed.shape
    width = LANES
    squares = {}
    for (mask, row), piece in zip(masks, pieces):
        here = slice(row, row + piece.shape[1])
        for z in range(piece.shape[0]):
            block = piece[z].astype(float32)
            owner = me ^ (mask + NEAR_Z * z)
            columns = pl.ds(pl.multiple_of(owner * width, width), width)
            normed[here, columns] = (block * gain_ref[:, columns]).astype(bfloat16)
            squares[row] = squares[row] + block * block if row in squares else block * block
    total = jnp.concatenate([squares[row] for row in sorted(squares)])
    scale = lax.rsqrt(jnp.sum(total, axis=1, keepdims=True) / depth + epsilon)
    across = (((1,), (1,)), ((), ()))
    gate, up = (
        scale * lax.dot_general(normed[...], weight[...], across, preferred_element_type=float32)
        for weight in (gate_ref, up_ref)
    )
    hidden = (gate * jax.nn.sigmoid(gate) * up).astype(bfloat16)
    low = (me & CORE) == 0
    for group, mask in enumerate((NEAR_X | NEAR_Y, NEAR_Y, NEAR_X, 0)):
        for z in range(keeps[group].shape[0]):
            pair = (me ^ (mask + NEAR_Z * z)) >> 1
            columns = pl.ds(pl.multiple_of(pair * 2 * width, 2 * width), 2 * width)
            both = jnp.dot(hidden, down_ref[:, columns], preferred_element_type=float32)
            left, right = both[:, :width], both[:, width:]
            keeps[group][z] = jnp.where(low, left, right)
            sends[group][z] = jnp.where(low, right, left).astype(bfloat16)


def half_partials(me, pieces, gain, gate, up, down, *seen):
    depth = gain.shape[0]
    z_count = device_count() // NEAR_Z
    masks = tuple((mask, row) for mask, row, _ in pieces)
    arrays = tuple(piece for _, _, piece in pieces) + seen
    rows = max(row + piece.shape[1] for _, row, piece in pieces)
    group = (z_count, rows, LANES)
    return pl.pallas_call(
        functools.partial(half_body, masks),
        out_shape=[jax.ShapeDtypeStruct(group, bfloat16)] * 4
        + [jax.ShapeDtypeStruct(group, float32)] * 4,
        in_specs=[SCALAR] + [WHOLE] * (4 + len(arrays)),
        out_specs=[WHOLE] * 8,
        scratch_shapes=[pltpu.VMEM((rows, depth), bfloat16)],
        compiler_params=params(24),
        name="half_step",
    )(me, gain.reshape(1, depth), gate, up, down, *arrays)


def scatter_sum(partials, count=1):
    sends, keeps = partials[:4], partials[4:]
    received = [flip(block, CORE) for block in sends]
    groups = [keep + block.astype(float32) for keep, block in zip(keeps, received)]
    *groups, owns = [stripes(group, 1, count) for group in groups]
    totals = []
    for index, own in enumerate(owns):
        for mask, group in zip((NEAR_X | NEAR_Y, NEAR_Y, NEAR_X), groups):
            moved = flip(group[index].astype(bfloat16), mask)
            own = own + moved.astype(float32)
        total = own[0]
        for z in range(1, own.shape[0]):
            moved = flip(own[z].astype(bfloat16), NEAR_Z * z)
            total = total + moved.astype(float32)
        totals.append(total)
    return jnp.concatenate(totals)


def project_body(me_ref, gain_ref, w0, w1, w2, w3, b0, b1, b2, b3, left_ref, right_ref, normed, sums):
    me = me_ref[0]
    kv, tp = me // 4, me % 4
    groups, own_rows, _ = left_ref.shape
    rows, _ = normed.shape
    squares = jnp.zeros((rows, LANES), float32)
    for mask, piece in enumerate((b0, b1, b2, b3)):
        values = piece[...].astype(float32)
        columns = pl.ds(pl.multiple_of((tp ^ mask) * LANES, LANES), LANES)
        wide = pl.ds(pl.multiple_of((me ^ mask) * LANES, LANES), LANES)
        normed[:, columns] = (values * gain_ref[:, wide]).astype(bfloat16)
        squares = squares + values * values
    total = jnp.sum(squares, axis=1, keepdims=True)
    coarse = total.astype(bfloat16).astype(float32)
    fine = total - coarse
    lane = lax.broadcasted_iota(jnp.int32, (rows, LANES), 1)
    square = jnp.where(lane < LANES // 2, coarse, fine)
    for weights, out_ref in (((w0, w1), left_ref), ((w2, w3), right_ref)):
        width = 0
        for weight in weights:
            sums[:, width : width + weight.shape[1]] = jnp.dot(
                normed[...], weight[...], preferred_element_type=float32
            )
            width += weight.shape[1]
        if width < out_ref.shape[2]:
            sums[:, width:] = square
            width += LANES
        for mask in range(groups):
            start = pl.multiple_of((kv ^ mask) * own_rows, own_rows)
            out_ref[mask] = sums[pl.ds(start, own_rows), :width].astype(bfloat16)


def project(me, blocks, mix_gain, weights, own_rows):
    rows = blocks[0].shape[0]
    block, width = weights[0].shape
    groups = rows // own_rows
    return pl.pallas_call(
        project_body,
        out_shape=[
            jax.ShapeDtypeStruct((groups, own_rows, 2 * width + extra), bfloat16)
            for extra in (LANES, 0)
        ],
        in_specs=[SCALAR] + [WHOLE] * 9,
        out_specs=[WHOLE] * 2,
        scratch_shapes=[
            pltpu.VMEM((rows, block), bfloat16),
            pltpu.VMEM((rows, 2 * width + LANES), float32),
        ],
        compiler_params=params(24),
        name="project",
    )(me, mix_gain.reshape(1, -1), *weights, *blocks)


def scatter_rows(left, right):
    bits = left.shape[0].bit_length() - 1
    parts = [block.reshape((2,) * bits + block.shape[1:]) for block in (left, right)]
    orders = [list(range(bits)), [1, 0] + list(range(2, bits))]
    crossed = [[], []]
    for step in range(bits):
        for side in range(2):
            bit = orders[side][step]
            later = [b for b in range(bits)[::-1] if b not in crossed[side]]
            axis = later.index(bit)
            part = parts[side]
            stay, leave = (
                lax.index_in_dim(part, half, axis, keepdims=False) for half in range(2)
            )
            moved = flip(leave.astype(bfloat16), NEAR_Y << bit)
            parts[side] = stay.astype(float32) + moved.astype(float32)
            crossed[side].append(bit)
    return jnp.concatenate(parts, axis=1)


def gates(sums_ref, here, floors, depth):
    inner = floors.shape[1]
    extra = 2 * inner
    squares = sums_ref[here, extra : extra + 1]
    squares = squares + sums_ref[here, extra + LANES // 2 : extra + LANES // 2 + 1]
    scale = lax.rsqrt(squares / depth + epsilon)
    query, forget, value, gate = (
        scale * sums_ref[here, start : start + inner]
        for start in (0, inner, extra + LANES, extra + LANES + inner)
    )
    kept = floors + (1.0 - floors) * jax.nn.sigmoid(forget)
    written = (1.0 - floors) * jax.nn.sigmoid(-forget)
    return query * jax.nn.sigmoid(query), kept, written, value, gate * jax.nn.sigmoid(gate)


def read_body(depth, sums_ref, floor_ref, gain_ref, past_ref, out_ref, mixed):
    own_rows, heads, size, _ = past_ref.shape
    rows = min(8, own_rows)
    floors = floor_ref[...]

    def some_rows(step, carry):
        here = pl.ds(pl.multiple_of(step * rows, rows), rows)
        query, kept, written, value, gate = gates(sums_ref, here, floors, depth)
        row = lax.broadcasted_iota(jnp.int32, (rows, size), 0)
        for h in range(heads):
            lanes = slice(h * size, (h + 1) * size)
            ask = query[:, lanes] * kept[:, lanes]
            coarse = ask.astype(bfloat16)
            fine = (ask - coarse.astype(float32)).astype(bfloat16)
            both = jnp.concatenate([coarse, fine])
            new = jnp.sum(query[:, lanes] * written[:, lanes], axis=1, keepdims=True)
            part = new * value[:, lanes]
            for n in range(rows):
                state = past_ref[step * rows + n, h]
                high = state.astype(bfloat16)
                low = (state - high.astype(float32)).astype(bfloat16)
                terms = jnp.dot(both, high, preferred_element_type=float32)
                terms = terms[:rows] + terms[rows:]
                terms = terms + jnp.dot(coarse, low, preferred_element_type=float32)
                part = part + jnp.where(row == n, terms, 0.0)
            power = jnp.mean(part * part, axis=1, keepdims=True)
            part = part * lax.rsqrt(power + epsilon) * gain_ref[...]
            mixed[here, lanes] = part * gate[:, lanes]
        return carry

    lax.fori_loop(0, own_rows // rows, some_rows, 0)
    out_ref[...] = mixed[...].astype(bfloat16)


def read(sums, forget_floor, head_gain, past_state, depth):
    own_rows, heads, size, _ = past_state.shape
    inner = heads * size
    return pl.pallas_call(
        functools.partial(read_body, depth),
        out_shape=jax.ShapeDtypeStruct((own_rows, inner), bfloat16),
        in_specs=[WHOLE] * 4,
        out_specs=WHOLE,
        scratch_shapes=[pltpu.VMEM((own_rows, inner), float32)],
        compiler_params=params(16),
        name="read",
    )(sums, forget_floor.reshape(1, inner), head_gain.reshape(1, size), past_state)


def update_body(depth, sums_ref, floor_ref, past_ref, new_ref):
    rows, heads, size, _ = past_ref.shape
    here = pl.ds(pl.multiple_of(pl.program_id(0) * rows, rows), rows)
    _, kept, written, value, _ = gates(sums_ref, here, floor_ref[...], depth)
    for h in range(heads):
        lanes = slice(h * size, (h + 1) * size)
        kept_t, written_t = kept[:, lanes].T, written[:, lanes].T
        for n in range(rows):
            column = slice(n, n + 1)
            new_ref[n, h] = (
                kept_t[:, column] * past_ref[n, h]
                + written_t[:, column] * value[column, lanes]
            )


def update(sums, forget_floor, past_state, depth):
    own_rows, heads, size, _ = past_state.shape
    rows = min(8, own_rows)
    inner = heads * size
    state = pl.BlockSpec((rows, heads, size, size), lambda i: (i, 0, 0, 0))
    return pl.pallas_call(
        functools.partial(update_body, depth),
        grid=(own_rows // rows,),
        out_shape=jax.ShapeDtypeStruct(past_state.shape, float32),
        in_specs=[
            pl.BlockSpec(sums.shape, lambda i: (0, 0)),
            pl.BlockSpec((1, inner), lambda i: (0, 0)),
            state,
        ],
        out_specs=state,
        compiler_params=params(16),
        cost_estimate=pl.CostEstimate(
            flops=2 * 10**9, bytes_accessed=8 * past_state.size, transcendentals=0
        ),
        name="update",
    )(sums, forget_floor.reshape(1, inner), past_state)


def gather_rows(own):
    z_count = lax.axis_size("kv") // 2
    column = stack([own] + [flip(own, NEAR_Z * z) for z in range(1, z_count)])
    return [column, flip(column, NEAR_Y)]


def mix_body(me_ref, weight_ref, near, far, *refs):
    outs, rows_ref = refs[:-1], refs[-1]
    me = me_ref[0]
    kv, tp = me // 4, me % 4
    own_rows = near.shape[1]
    for side, pieces in enumerate((near, far)):
        for z in range(pieces.shape[0]):
            start = pl.multiple_of((kv ^ (2 * z + side)) * own_rows, own_rows)
            rows_ref[pl.ds(start, own_rows), :] = pieces[z]
    for mask, out in enumerate(outs):
        columns = pl.ds(pl.multiple_of((tp ^ mask) * LANES, LANES), LANES)
        out[...] = jnp.dot(
            rows_ref[...], weight_ref[:, columns], preferred_element_type=float32
        ).astype(bfloat16)


def mix(me, pieces, weight):
    count, own_rows, width = pieces[0].shape
    rows = 2 * count * own_rows
    blocks = weight.shape[1] // LANES
    return pl.pallas_call(
        mix_body,
        out_shape=[jax.ShapeDtypeStruct((rows, LANES), bfloat16)] * blocks,
        in_specs=[SCALAR] + [WHOLE] * 3,
        out_specs=[WHOLE] * blocks,
        scratch_shapes=[pltpu.VMEM((rows, width), bfloat16)],
        compiler_params=params(16),
        name="mix",
    )(me, weight, *pieces)


def exchanged(
    tokens,
    past_state,
    pre_gain,
    pre_gate,
    pre_up,
    pre_down,
    mix_gain,
    query_weight,
    forget_weight,
    value_weight,
    output_gate_weight,
    forget_floor,
    head_gain,
    proj_out,
    post_gain,
    post_gate,
    post_up,
    post_down,
):
    me = lax.axis_index(AXES).astype(jnp.int32).reshape(1)
    me, tokens = lax.optimization_barrier((me, tokens))
    depth = pre_gain.shape[0]
    pieces = gather_all(tokens)
    weights = (pre_gate.T, pre_up.T, pre_down)
    seen = visit(*weights)
    partials = half_partials(me, pieces, pre_gain, *weights, seen)
    first = (tokens.astype(float32) + 0.5 * scatter_sum(partials)).astype(bfloat16)
    blocks = [first] + [flip(first, mask) for mask in (CORE, NEAR_X, NEAR_X | CORE)]
    weights = (query_weight, forget_weight, value_weight, output_gate_weight)
    own_rows = past_state.shape[0]
    sums = scatter_rows(*project(me, blocks, mix_gain, weights, own_rows))
    mixed_in = read(sums, forget_floor, head_gain, past_state, depth)
    new_state = update(sums, forget_floor, past_state, depth)
    parts = mix(me, gather_rows(mixed_in), proj_out)
    mixed = parts[0].astype(float32)
    for mask in (NEAR_X, NEAR_X | CORE, CORE):
        mixed = mixed + flip(parts[mask], mask).astype(float32)
    second = (first.astype(float32) + mixed).astype(bfloat16)
    pieces = gather_all(second, 2)
    weights = (post_gate.T, post_up.T, post_down)
    partials = half_partials(me, pieces, post_gain, *weights)
    result = (second.astype(float32) + 0.5 * scatter_sum(partials)).astype(bfloat16)
    return (result, new_state)


def half_inputs(activations, gain, w_gate, w_up):
    piece_float = lax.all_gather(activations, ("kv", "tp"), axis=1, tiled=True).astype(jnp.float32)
    normed = (piece_float * gain).astype(jnp.bfloat16)
    gate_acc = jnp.dot(normed, w_gate, preferred_element_type=jnp.float32)
    up_acc = jnp.dot(normed, w_up, preferred_element_type=jnp.float32)
    squares = jnp.sum(piece_float * piece_float, axis=1)
    row_scale = lax.rsqrt(squares / piece_float.shape[1] + epsilon)[:, None]
    return (jax.nn.silu(row_scale * gate_acc) * (row_scale * up_acc)).astype(jnp.bfloat16)


def down_sum(hidden, w_down):
    return lax.psum_scatter(
        jnp.dot(hidden, w_down, preferred_element_type=jnp.float32),
        ("kv", "tp"),
        scatter_dimension=1,
        tiled=True,
    )


def per_device(
    tokens,
    past_state,
    pre_gain,
    pre_gate,
    pre_up,
    pre_down,
    mix_gain,
    query_weight,
    forget_weight,
    value_weight,
    output_gate_weight,
    forget_floor,
    head_gain,
    proj_out,
    post_gain,
    post_gate,
    post_up,
    post_down,
):
    whole_rows = lax.all_gather(tokens, ("kv", "tp"), axis=1, tiled=True)
    whole_float = whole_rows.astype(jnp.float32)
    row_scale = lax.rsqrt(jnp.mean(whole_float * whole_float, axis=1, keepdims=True) + epsilon)
    normed = (whole_float * pre_gain).astype(jnp.bfloat16)
    gate_pre = row_scale * jnp.dot(normed, pre_gate, preferred_element_type=jnp.float32)
    up_pre = row_scale * jnp.dot(normed, pre_up, preferred_element_type=jnp.float32)
    hidden = (jax.nn.silu(gate_pre) * up_pre).astype(jnp.bfloat16)
    kv_sums = lax.psum_scatter(
        jnp.dot(hidden, pre_down, preferred_element_type=jnp.float32).astype(jnp.bfloat16),
        "kv",
        scatter_dimension=1,
        tiled=True,
    )
    block_sum = lax.psum(kv_sums, "tp").astype(jnp.float32)
    block_width = block_sum.shape[1]
    block_old = lax.dynamic_slice_in_dim(
        whole_rows, lax.axis_index("kv") * block_width, block_width, 1
    )
    block_rows = (block_old.astype(jnp.float32) + 0.5 * block_sum).astype(jnp.bfloat16)
    own_width = block_width // lax.axis_size("tp")
    after_first = lax.dynamic_slice_in_dim(
        block_rows, lax.axis_index("tp") * own_width, own_width, 1
    )
    block_width = block_rows.shape[1]
    block_float = block_rows.astype(jnp.float32)
    block_gain = lax.dynamic_slice_in_dim(
        mix_gain, lax.axis_index("kv") * block_width, block_width, 0
    )
    squares = lax.psum(jnp.sum(block_float * block_float, axis=1), "kv")
    normed = (block_float * block_gain).astype(jnp.bfloat16)
    own_rows = past_state.shape[0]
    weight_list = (query_weight, forget_weight, value_weight, output_gate_weight)
    projected = lax.psum_scatter(
        jnp.concatenate(
            [
                jnp.dot(normed, weight_part, preferred_element_type=jnp.float32)
                for weight_part in weight_list
            ],
            axis=1,
        ).astype(jnp.bfloat16),
        "kv",
        scatter_dimension=0,
        tiled=True,
    ).astype(jnp.float32)
    own_squares = lax.dynamic_slice_in_dim(squares, lax.axis_index("kv") * own_rows, own_rows, 0)
    projected = projected * lax.rsqrt(own_squares / pre_gain.shape[0] + epsilon)[:, None]
    pre_query, pre_forget, pre_value, pre_gate_out = jnp.split(projected, 4, axis=1)
    local_heads = past_state.shape[1]
    head_width = past_state.shape[2]
    head_shape = (own_rows, local_heads, head_width)
    floors = forget_floor.reshape(local_heads, head_width)
    forget_heads = pre_forget.reshape(head_shape)
    forget = floors + (1.0 - floors) * jax.nn.sigmoid(forget_heads)
    written = (1.0 - floors) * jax.nn.sigmoid(-forget_heads)
    query_act = jax.nn.silu(pre_query.reshape(head_shape))
    value_act = pre_value.reshape(head_shape)
    new_state = (
        forget[:, :, :, None] * past_state + written[:, :, :, None] * value_act[:, :, None, :]
    )
    readout = jnp.einsum("bhkv,bhk->bhv", new_state, query_act, precision=lax.Precision.HIGHEST)
    readout = (
        readout
        * lax.rsqrt(jnp.mean(readout * readout, axis=2, keepdims=True) + epsilon)
        * head_gain
    )
    mixed_in = (
        readout.reshape(own_rows, local_heads * head_width) * jax.nn.silu(pre_gate_out)
    ).astype(jnp.bfloat16)
    partials = jnp.dot(
        lax.all_gather(mixed_in, "kv", axis=0, tiled=True),
        proj_out,
        preferred_element_type=jnp.float32,
    ).astype(jnp.bfloat16)
    mixed_sum = lax.psum_scatter(partials, "tp", scatter_dimension=1, tiled=True).astype(
        jnp.float32
    )
    second = (after_first.astype(jnp.float32) + mixed_sum).astype(jnp.bfloat16)
    hidden_two = half_inputs(second, post_gain, post_gate, post_up)
    result = (second.astype(jnp.float32) + 0.5 * down_sum(hidden_two, post_down)).astype(
        jnp.bfloat16
    )
    return (result, new_state)


def solution(mesh):
    placed = (
        P(None, ("kv", "tp")),
        P("kv", "tp", None, None),
        P(),
        P(None, ("kv", "tp")),
        P(None, ("kv", "tp")),
        P(("kv", "tp"), None),
        P(),
        P("kv", "tp"),
        P("kv", "tp"),
        P("kv", "tp"),
        P("kv", "tp"),
        P("tp"),
        P(),
        P("tp", "kv"),
        P(),
        P(None, ("kv", "tp")),
        P(None, ("kv", "tp")),
        P(("kv", "tp"), None),
    )

    def local(*arrays):
        width = arrays[0].shape[1]
        fits = mesh.shape["tp"] == 4 and mesh.shape["kv"] in (4, 8, 16)
        plan = exchanged if fits and width == LANES else per_device
        return plan(*arrays)

    return jax.shard_map(
        local,
        mesh=mesh,
        in_specs=placed,
        out_specs=(P(None, ("kv", "tp")), P("kv", "tp", None, None)),
        check_vma=False,
    )
```

time: 208 us -> 176 us (0.85)
  waiting for transfers between devices: 101 us -> 77.9 us
  local copies, waits for them, and re-layouts: 27.5 us -> 9.25 us
  starting transfers between devices: 51.7 us -> 63.4 us
    ppermute x59 -> x66, waiting for transfers between devices: 101 us -> 77.9 us  [flip(): return lax.ppermute(block, AXES, pairs)]
    unnamed x42 -> x46, local copies, waits for them, and re-layouts: 23.6 us -> 9.06 us
    ppermute x59 -> x66, starting transfers between devices: 51.7 us -> 63.4 us  [flip(): return lax.ppermute(block, AXES, pairs)]
    slice x10 -> x2, local copies, waits for them, and re-layouts: 3.78 us -> 0.08 us  [scatter_rows(): lax.index_in_dim(part, half, axis, keepdims=False)]
    pallas_call x2, Pallas kernels: 11.4 us -> 8.63 us  [half_partials(): pl.pallas_call(functools.partial(half_body, masks), out_shape=[jax.ShapeD...]
    pallas_call x3 -> x5, Pallas kernels: 10.9 us -> 12.6 us  [the longest x1 7.54 us: update(): pl.pallas_call(functools.partial(update_body, depth), grid=(own_rows // r...]
  transfers between devices with their start and end apart: 59 -> 66, of which waited for: 38 -> 33; matrix products, arithmetic and copies ran while one was open for 10% -> 0% of each run, Pallas kernels for 0% -> 4%
where the time goes in v2:
time: 176 us
  waiting for transfers between devices  77.9 us (44%)
  starting transfers between devices  63.4 us (36%)
  Pallas kernels  21.2 us (12%)
  local copies, waits for them, and re-layouts  9.25 us (5%)
  other arithmetic  2.66 us (2%)
    ppermute x66, waiting for transfers between devices, flip(): return lax.ppermute(block, AXES, pairs)  77.9 us
    ppermute x66, starting transfers between devices, flip(): return lax.ppermute(block, AXES, pairs)  63.4 us
    unnamed x46, local copies, waits for them, and re-layouts  9.06 us
    pallas_call x2, Pallas kernels, half_partials(): pl.pallas_call(functools.partial(half_body, masks), out_shape=[jax.ShapeD...  8.63 us
    pallas_call x1, Pallas kernels, update(): pl.pallas_call(functools.partial(update_body, depth), grid=(own_rows // r...  7.54 us
    pallas_call x1, Pallas kernels, read(): pl.pallas_call(functools.partial(read_body, depth), out_shape=jax.ShapeDt...  3.76 us
  transfers between devices with their start and end apart: 66, of which 33 were waited for; matrix products, arithmetic and copies ran while one was open for 0% of the time, Pallas kernels for 4%

profile of v2, /device:TPU:0, one launch (start us, length us, event | category | flops | bytes accessed | tf_op | source)
XLA Modules:
  0.0 175.7 jit_solution(5617459751891765261)
XLA Ops:
  0.6 5.1 %collective-permute-start.2 = (bf16[256,128]{1,0:T(8,128)(2,1)}, bf16[256,128]{1,0:T(8,128)(2,1)S(1)}, u32[]{:S(2)}, u32[]{:S(2)}) collective-permute-start(bf16[256,128]{1,0:T(8,128)(2,1)} %param.18), channel_id=1, source_target_pairs={{0,24},{1,25},{2,26},{3,27},{4,28},{5,29},{6,30},{7,31},{8,16},{9,... | collective-permute-start | bytes 196616 | tf_op jit(solution)/shard_map/ppermute | solution.py:30
  8.6 3.0 %collective-permute-done.1 = bf16[256,128]{1,0:T(8,128)(2,1)S(1)} collective-permute-done((bf16[256,128]{1,0:T(8,128)(2,1)}, bf16[256,128]{1,0:T(8,128)(2,1)S(1)}, u32[]{:S(2)}, u32[]{:S(2)}) %collective-permute-start.1) | collective-permute-done | bytes 65568 | tf_op jit(solution)/shard_map/ppermute | solution.py:30
  16.0 5.7 %collective-permute-done.5.refs_3_ = bf16[4,256,128]{2,1,0:T(8,128)(2,1)S(1)} collective-permute-done((bf16[4,256,128]{2,1,0:T(8,128)(2,1)S(1)}, bf16[4,256,128]{2,1,0:T(8,128)(2,1)S(1)}, u32[]{:S(2)}, u32[]{:S(2)}) %collective-permute-start.5) | collective-permute-done | bytes 262176 | tf_op jit(solution)/shard_map/ppermute | solution.py:30
  21.7 5.6 %collective-permute-done.4.refs_2_ = bf16[4,256,128]{2,1,0:T(8,128)(2,1)S(1)} collective-permute-done((bf16[4,256,128]{2,1,0:T(8,128)(2,1)S(1)}, bf16[4,256,128]{2,1,0:T(8,128)(2,1)S(1)}, u32[]{:S(2)}, u32[]{:S(2)}) %collective-permute-start.4) | collective-permute-done | bytes 262176 | tf_op jit(solution)/shard_map/ppermute | solution.py:30
  36.9 4.4 %half_step.2 = (bf16[4,256,128]{2,1,0:T(8,128)(2,1)S(1)}, bf16[4,256,128]{2,1,0:T(8,128)(2,1)S(1)}, bf16[4,256,128]{2,1,0:T(8,128)(2,1)S(1)}, bf16[4,256,128]{2,...) custom-call(s32[1]{0:T(128)} %bitcast.me_ref, ...), custom_call_target="tpu_custom_call" | custom-call | tf_op jit(solution)/shard_map/half_step/pallas_call | solution.py:113
  46.8 6.4 %collective-permute-done.12 = bf16[4,256,128]{2,1,0:T(8,128)(2,1)S(1)} collective-permute-done((bf16[4,256,128]{2,1,0:T(8,128)(2,1)S(1)}, bf16[4,256,128]{2,1,0:T(8,128)(2,1)S(1)}, u32[]{:S(2)}, u32[]{:S(2)}) %collective-permute-start.12) | collective-permute-done | bytes 262176 | tf_op jit(solution)/shard_map/ppermute | solution.py:30
  53.2 4.7 %collective-permute-done.14 = bf16[4,256,128]{2,1,0:T(8,128)(2,1)S(1)} collective-permute-done((bf16[4,256,128]{2,1,0:T(8,128)(2,1)S(1)}, bf16[4,256,128]{2,1,0:T(8,128)(2,1)S(1)}, u32[]{:S(2)}, u32[]{:S(2)}) %collective-permute-start.14) | collective-permute-done | bytes 262176 | tf_op jit(solution)/shard_map/ppermute | solution.py:30
  62.5 2.3 %collective-permute-done.19 = bf16[256,128]{1,0:T(8,128)(2,1)S(1)} collective-permute-done((bf16[256,128]{1,0:T(8,128)(2,1)S(1)}, bf16[256,128]{1,0:T(8,128)(2,1)S(1)}, u32[]{:S(2)}, u32[]{:S(2)}) %collective-permute-start.19) | collective-permute-done | bytes 65568 | tf_op jit(solution)/shard_map/ppermute | solution.py:30
  64.9 2.7 %collective-permute-done.18 = bf16[256,128]{1,0:T(8,128)(2,1)S(1)} collective-permute-done((bf16[256,128]{1,0:T(8,128)(2,1)S(1)}, bf16[256,128]{1,0:T(8,128)(2,1)S(1)}, u32[]{:S(2)}, u32[]{:S(2)}) %collective-permute-start.18) | collective-permute-done | bytes 65568 | tf_op jit(solution)/shard_map/ppermute | solution.py:30
  69.6 2.5 %collective-permute-done.22.b3 = bf16[256,128]{1,0:T(8,128)(2,1)S(1)} collective-permute-done((bf16[256,128]{1,0:T(8,128)(2,1)S(1)}, bf16[256,128]{1,0:T(8,128)(2,1)S(1)}, u32[]{:S(2)}, u32[]{:S(2)}) %collective-permute-start.22) | collective-permute-done | bytes 65568 | tf_op jit(solution)/shard_map/ppermute | solution.py:30
  75.5 6.8 %collective-permute-done.26 = bf16[2,2,32,1024]{3,2,0,1:T(8,128)(2,1)S(1)} collective-permute-done((bf16[2,2,32,1024]{3,2,0,1:T(8,128)(2,1)S(1)}, bf16[2,2,32,1024]{3,2,0,1:T(8,128)(2,1)S(1)}, u32[]{:S(2)}, u32[]{:S(2)}) %collective-permute-start.26) | collective-permute-done | bytes 262176 | tf_op jit(solution)/shard_map/ppermute | solution.py:30
  85.0 2.3 %collective-permute-done.27 = bf16[2,32,1024]{2,1,0:T(8,128)(2,1)S(1)} collective-permute-done((bf16[2,32,1024]{2,1,0:T(8,128)(2,1)S(1)}, bf16[2,32,1024]{2,1,0:T(8,128)(2,1)S(1)}, u32[]{:S(2)}, u32[]{:S(2)}) %collective-permute-start.27) | collective-permute-done | bytes 131104 | tf_op jit(solution)/shard_map/ppermute | solution.py:30
  89.1 2.4 %collective-permute-start.25 = (bf16[32,1152]{1,0:T(8,128)(2,1)S(1)}, bf16[32,1152]{1,0:T(8,128)(2,1)S(1)}, u32[]{:S(2)}, u32[]{:S(2)}) collective-permute-start(bf16[32,1152]{1,0:T(8,128)(2,1)S(1)} %fusion.18), channel_id=1, source_target_pairs={{0,16},{1,17},{2,18},{3,19},{4,20},{5,21},{6,22},{7,23},{8,24},{9,... | collective-permute-start | bytes 221192 | tf_op jit(solution)/shard_map/ppermute | solution.py:30
  91.5 2.3 %collective-permute-done.28 = bf16[32,1024]{1,0:T(8,128)(2,1)S(1)} collective-permute-done((bf16[32,1024]{1,0:T(8,128)(2,1)S(1)}, bf16[32,1024]{1,0:T(8,128)(2,1)S(1)}, u32[]{:S(2)}, u32[]{:S(2)}) %collective-permute-start.28) | collective-permute-done | bytes 65568 | tf_op jit(solution)/shard_map/ppermute | solution.py:30
  94.8 3.8 %read.1 = bf16[32,512]{1,0:T(8,128)(2,1)S(1)} custom-call(f32[32,2176]{1,0:T(8,128)S(1)} %pad_maximum_fusion.sums_ref, f32[1,512]{1,0:T(1,128)S(1)} %bitcast.124, f32[1,128]{1,0:T(1,128)S(1)} %bitcast.126, f32[32,4,128,128]{3,2,1,0:T(8,128)S(1)} %bitcast.111), custom_call_target="tpu_custom_call" | custom-call | tf_op jit(solution)/shard_map/read/pallas_call | solution.py:268
  107.1 3.8 %collective-permute-done.32.far = bf16[4,32,512]{2,1,0:T(8,128)(2,1)S(1)} collective-permute-done((bf16[4,32,512]{2,1,0:T(8,128)(2,1)S(1)}, bf16[4,32,512]{2,1,0:T(8,128)(2,1)S(1)}, u32[]{:S(2)}, u32[]{:S(2)}) %collective-permute-start.32) | collective-permute-done | bytes 131104 | tf_op jit(solution)/shard_map/ppermute | solution.py:30
  121.9 2.3 %collective-permute-start.46 = (bf16[128,128]{1,0:T(8,128)(2,1)S(1)}, bf16[128,128]{1,0:T(8,128)(2,1)S(1)}, u32[]{:S(2)}, u32[]{:S(2)}) collective-permute-start(bf16[128,128]{1,0:T(8,128)(2,1)S(1)} %get-tuple-element.66), channel_id=1, source_target_pairs={{0,8},{1,9},{2,10},{3,11},{4,12},{5,13},{6,14},{7,15},{8,0},{9,1},... | collective-permute-start | bytes 98312 | tf_op jit(solution)/shard_map/ppermute | solution.py:30
  133.7 4.1 %collective-permute-start.49 = (bf16[4,128,128]{2,1,0:T(8,128)(2,1)S(1)}, bf16[4,128,128]{2,1,0:T(8,128)(2,1)S(1)}, u32[]{:S(2)}, u32[]{:S(2)}) collective-permute-start(bf16[4,128,128]{2,1,0:T(8,128)(2,1)S(1)} %pad_maximum_fusion.4.refs_8_), channel_id=1, source_target_pairs={{0,6},{1,7},{2,4},{3,5},{4,2},{5,3},{6,0},{7,1},{8,14},{9,15},{10,... | collective-permute-start | bytes 393224 | tf_op jit(solution)/shard_map/ppermute | solution.py:30
  138.8 2.2 %collective-permute-done.49.refs_9_ = bf16[4,128,128]{2,1,0:T(8,128)(2,1)S(1)} collective-permute-done((bf16[4,128,128]{2,1,0:T(8,128)(2,1)S(1)}, bf16[4,128,128]{2,1,0:T(8,128)(2,1)S(1)}, u32[]{:S(2)}, u32[]{:S(2)}) %collective-permute-start.49) | collective-permute-done | bytes 131104 | tf_op jit(solution)/shard_map/ppermute | solution.py:30
  142.6 4.3 %half_step.3 = (bf16[4,256,128]{2,1,0:T(8,128)(2,1)S(1)}, bf16[4,256,128]{2,1,0:T(8,128)(2,1)S(1)}, bf16[4,256,128]{2,1,0:T(8,128)(2,1)S(1)}, bf16[4,256,128]{2,...) custom-call(s32[1]{0:T(128)} %bitcast.me_ref, ...), custom_call_target="tpu_custom_call" | custom-call | tf_op jit(solution)/shard_map/half_step/pallas_call | solution.py:113
  148.6 2.7 %collective-permute-start.58 = (bf16[4,256,128]{2,1,0:T(8,128)(2,1)S(1)}, bf16[4,256,128]{2,1,0:T(8,128)(2,1)S(1)}, u32[]{:S(2)}, u32[]{:S(2)}) collective-permute-start(bf16[4,256,128]{2,1,0:T(8,128)(2,1)S(1)} %add_convert_fusion.2), channel_id=1, source_target_pairs={{0,6},{1,7},{2,4},{3,5},{4,2},{5,3},{6,0},{7,1},{8,14},{9,15},{10,... | collective-permute-start | bytes 786440 | tf_op jit(solution)/shard_map/ppermute | solution.py:30
  152.4 6.4 %collective-permute-done.58 = bf16[4,256,128]{2,1,0:T(8,128)(2,1)S(1)} collective-permute-done((bf16[4,256,128]{2,1,0:T(8,128)(2,1)S(1)}, bf16[4,256,128]{2,1,0:T(8,128)(2,1)S(1)}, u32[]{:S(2)}, u32[]{:S(2)}) %collective-permute-start.58) | collective-permute-done | bytes 262176 | tf_op jit(solution)/shard_map/ppermute | solution.py:30
  158.7 4.9 %collective-permute-done.60 = bf16[4,256,128]{2,1,0:T(8,128)(2,1)S(1)} collective-permute-done((bf16[4,256,128]{2,1,0:T(8,128)(2,1)S(1)}, bf16[4,256,128]{2,1,0:T(8,128)(2,1)S(1)}, u32[]{:S(2)}, u32[]{:S(2)}) %collective-permute-start.60) | collective-permute-done | bytes 262176 | tf_op jit(solution)/shard_map/ppermute | solution.py:30
  167.4 7.5 %update.1 = f32[32,4,128,128]{3,2,1,0:T(8,128)} custom-call(f32[32,2176]{1,0:T(8,128)S(1)} %pad_maximum_fusion.sums_ref, f32[1,512]{1,0:T(1,128)S(1)} %bitcast.125, f32[32,4,128,128]{3,2,1,0:T(8,128)S(1)} %bitcast.111), custom_call_target="tpu_custom_call" | custom-call | flops 2000000000 | bytes 16777216 | tf_op jit(solution)/shard_map/update/pallas_call | solution.py:299
  (193 shorter events, 76.2 us)
Async XLA Ops:
  0.6 7.9 %collective-permute-start.2 = (bf16[256,128]{1,0:T(8,128)(2,1)}, bf16[256,128]{1,0:T(8,128)(2,1)S(1)}, u32[]{:S(2)}, u32[]{:S(2)}) collective-permute-start(bf16[256,128]{1,0:T(8,128)(2,1)} %param.18), channel_id=1, source_target_pairs={{0,24},{1,25},{2,26},{3,27},{4,28},{5,29},{6,30},{7,31},{8,16},{9,... | collective-permute-start | bytes 196616 | tf_op jit(solution)/shard_map/ppermute | solution.py:30
  12.5 9.2 %collective-permute-start.5 = (bf16[4,256,128]{2,1,0:T(8,128)(2,1)S(1)}, bf16[4,256,128]{2,1,0:T(8,128)(2,1)S(1)}, u32[]{:S(2)}, u32[]{:S(2)}) collective-permute-start(bf16[4,256,128]{2,1,0:T(8,128)(2,1)S(1)} %pad_maximum_fusion.1.refs_0_), channel_id=1, source_target_pairs={{0,2},{1,3},{2,0},{3,1},{4,6},{5,7},{6,4},{7,5},{8,10},{9,11},{10,... | collective-permute-start | bytes 786440 | tf_op jit(solution)/shard_map/ppermute | solution.py:30
  14.0 13.3 %collective-permute-start.4 = (bf16[4,256,128]{2,1,0:T(8,128)(2,1)S(1)}, bf16[4,256,128]{2,1,0:T(8,128)(2,1)S(1)}, u32[]{:S(2)}, u32[]{:S(2)}) collective-permute-start(bf16[4,256,128]{2,1,0:T(8,128)(2,1)S(1)} %pad_maximum_fusion.1.refs_0_), channel_id=1, source_target_pairs={{0,4},{1,5},{2,6},{3,7},{4,0},{5,1},{6,2},{7,3},{8,12},{9,13},{10,... | collective-permute-start | bytes 786440 | tf_op jit(solution)/shard_map/ppermute | solution.py:30
  15.6 11.8 %collective-permute-start.3 = (bf16[4,256,128]{2,1,0:T(8,128)(2,1)S(1)}, bf16[4,256,128]{2,1,0:T(8,128)(2,1)S(1)}, u32[]{:S(2)}, u32[]{:S(2)}) collective-permute-start(bf16[4,256,128]{2,1,0:T(8,128)(2,1)S(1)} %pad_maximum_fusion.1.refs_0_), channel_id=1, source_target_pairs={{0,6},{1,7},{2,4},{3,5},{4,2},{5,3},{6,0},{7,1},{8,14},{9,15},{10,... | collective-permute-start | bytes 786440 | tf_op jit(solution)/shard_map/ppermute | solution.py:30
  16.0 17.3 %collective-permute-start.6 = (bf16[4,256,128]{2,1,0:T(8,128)(2,1)S(1)}, bf16[4,256,128]{2,1,0:T(8,128)(2,1)S(1)}, u32[]{:S(2)}, u32[]{:S(2)}) collective-permute-start(bf16[4,256,128]{2,1,0:T(8,128)(2,1)S(1)} %pad_maximum_fusion.1.refs_0_), channel_id=1, source_target_pairs={{0,1},{1,0},{2,3},{3,2},{4,5},{5,4},{6,7},{7,6},{8,9},{9,8},{10,11... | collective-permute-start | bytes 786440 | tf_op jit(solution)/shard_map/ppermute | solution.py:30
  21.7 11.6 %collective-permute-start.9 = (bf16[4,256,128]{2,1,0:T(8,128)(2,1)S(1)}, bf16[4,256,128]{2,1,0:T(8,128)(2,1)S(1)}, u32[]{:S(2)}, u32[]{:S(2)}) collective-permute-start(bf16[4,256,128]{2,1,0:T(8,128)(2,1)S(1)} %collective-permute-done.5.refs_3_), channel_id=1, source_target_pairs={{0,1},{1,0},{2,3},{3,2},{4,5},{5,4},{6,7},{7,6},{8,9},{9,8},{10,11... | collective-permute-start | bytes 786440 | tf_op jit(solution)/shard_map/ppermute | solution.py:30
  43.0 10.2 %collective-permute-start.12 = (bf16[4,256,128]{2,1,0:T(8,128)(2,1)S(1)}, bf16[4,256,128]{2,1,0:T(8,128)(2,1)S(1)}, u32[]{:S(2)}, u32[]{:S(2)}) collective-permute-start(bf16[4,256,128]{2,1,0:T(8,128)(2,1)S(1)} %add_convert_fusion.5), channel_id=1, source_target_pairs={{0,6},{1,7},{2,4},{3,5},{4,2},{5,3},{6,0},{7,1},{8,14},{9,15},{10,... | collective-permute-start | bytes 786440 | tf_op jit(solution)/shard_map/ppermute | solution.py:30
  44.6 13.3 %collective-permute-start.14 = (bf16[4,256,128]{2,1,0:T(8,128)(2,1)S(1)}, bf16[4,256,128]{2,1,0:T(8,128)(2,1)S(1)}, u32[]{:S(2)}, u32[]{:S(2)}) collective-permute-start(bf16[4,256,128]{2,1,0:T(8,128)(2,1)S(1)} %add_convert_fusion.4), channel_id=1, source_target_pairs={{0,4},{1,5},{2,6},{3,7},{4,0},{5,1},{6,2},{7,3},{8,12},{9,13},{10,... | collective-permute-start | bytes 786440 | tf_op jit(solution)/shard_map/ppermute | solution.py:30
  45.5 12.5 %collective-permute-start.16 = (bf16[4,256,128]{2,1,0:T(8,128)(2,1)S(1)}, bf16[4,256,128]{2,1,0:T(8,128)(2,1)S(1)}, u32[]{:S(2)}, u32[]{:S(2)}) collective-permute-start(bf16[4,256,128]{2,1,0:T(8,128)(2,1)S(1)} %add_convert_fusion.3), channel_id=1, source_target_pairs={{0,2},{1,3},{2,0},{3,1},{4,6},{5,7},{6,4},{7,5},{8,10},{9,11},{10,... | collective-permute-start | bytes 786440 | tf_op jit(solution)/shard_map/ppermute | solution.py:30
  60.0 7.6 %collective-permute-start.18 = (bf16[256,128]{1,0:T(8,128)(2,1)S(1)}, bf16[256,128]{1,0:T(8,128)(2,1)S(1)}, u32[]{:S(2)}, u32[]{:S(2)}) collective-permute-start(bf16[256,128]{1,0:T(8,128)(2,1)S(1)} %get-tuple-element.63), channel_id=1, source_target_pairs={{0,16},{1,17},{2,18},{3,19},{4,20},{5,21},{6,22},{7,23},{8,24},{9,... | collective-permute-start | bytes 196616 | tf_op jit(solution)/shard_map/ppermute | solution.py:30
  73.8 8.5 %collective-permute-start.26 = (bf16[2,2,32,1024]{3,2,0,1:T(8,128)(2,1)S(1)}, bf16[2,2,32,1024]{3,2,0,1:T(8,128)(2,1)S(1)}, u32[]{:S(2)}, u32[]{:S(2)}) collective-permute-start(bf16[2,2,32,1024]{3,2,0,1:T(8,128)(2,1)S(1)} %bitcast.128), channel_id=1, source_target_pairs={{0,8},{1,9},{2,10},{3,11},{4,12},{5,13},{6,14},{7,15},{8,0},{9,1},... | collective-permute-start | bytes 786440 | tf_op jit(solution)/shard_map/ppermute | solution.py:30
  74.0 9.8 %collective-permute-start.23 = (bf16[2,2,32,1152]{3,2,0,1:T(8,128)(2,1)S(1)}, bf16[2,2,32,1152]{3,2,0,1:T(8,128)(2,1)S(1)}, u32[]{:S(2)}, u32[]{:S(2)}) collective-permute-start(bf16[2,2,32,1152]{3,2,0,1:T(8,128)(2,1)S(1)} %bitcast.127), channel_id=1, source_target_pairs={{0,4},{1,5},{2,6},{3,7},{4,0},{5,1},{6,2},{7,3},{8,12},{9,13},{10,... | collective-permute-start | bytes 884744 | tf_op jit(solution)/shard_map/ppermute | solution.py:30
  117.1 7.1 %collective-permute-start.37 = (bf16[128,128]{1,0:T(8,128)(2,1)S(1)}, bf16[128,128]{1,0:T(8,128)(2,1)S(1)}, u32[]{:S(2)}, u32[]{:S(2)}) collective-permute-start(bf16[128,128]{1,0:T(8,128)(2,1)S(1)} %get-tuple-element.67), channel_id=1, source_target_pairs={{0,16},{1,17},{2,18},{3,19},{4,20},{5,21},{6,22},{7,23},{8,24},{9,... | collective-permute-start | bytes 98312 | tf_op jit(solution)/shard_map/ppermute | solution.py:30
  118.4 7.6 %collective-permute-start.36 = (bf16[128,128]{1,0:T(8,128)(2,1)S(1)}, bf16[128,128]{1,0:T(8,128)(2,1)S(1)}, u32[]{:S(2)}, u32[]{:S(2)}) collective-permute-start(bf16[128,128]{1,0:T(8,128)(2,1)S(1)} %get-tuple-element.67), channel_id=1, source_target_pairs={{0,8},{1,9},{2,10},{3,11},{4,12},{5,13},{6,14},{7,15},{8,0},{9,1},... | collective-permute-start | bytes 98312 | tf_op jit(solution)/shard_map/ppermute | solution.py:30
  128.1 9.7 %collective-permute-start.39 = (bf16[4,128,128]{2,1,0:T(8,128)(2,1)S(1)}, bf16[4,128,128]{2,1,0:T(8,128)(2,1)S(1)}, u32[]{:S(2)}, u32[]{:S(2)}) collective-permute-start(bf16[4,128,128]{2,1,0:T(8,128)(2,1)S(1)} %pad_maximum_fusion.3.refs_0_), channel_id=1, source_target_pairs={{0,6},{1,7},{2,4},{3,5},{4,2},{5,3},{6,0},{7,1},{8,14},{9,15},{10,... | collective-permute-start | bytes 393224 | tf_op jit(solution)/shard_map/ppermute | solution.py:30
  130.0 7.8 %collective-permute-start.52 = (bf16[4,128,128]{2,1,0:T(8,128)(2,1)S(1)}, bf16[4,128,128]{2,1,0:T(8,128)(2,1)S(1)}, u32[]{:S(2)}, u32[]{:S(2)}) collective-permute-start(bf16[4,128,128]{2,1,0:T(8,128)(2,1)S(1)} %pad_maximum_fusion.4.refs_8_), channel_id=1, source_target_pairs={{0,1},{1,0},{2,3},{3,2},{4,5},{5,4},{6,7},{7,6},{8,9},{9,8},{10,11... | collective-permute-start | bytes 393224 | tf_op jit(solution)/shard_map/ppermute | solution.py:30
  130.1 8.2 %collective-permute-start.51 = (bf16[4,128,128]{2,1,0:T(8,128)(2,1)S(1)}, bf16[4,128,128]{2,1,0:T(8,128)(2,1)S(1)}, u32[]{:S(2)}, u32[]{:S(2)}) collective-permute-start(bf16[4,128,128]{2,1,0:T(8,128)(2,1)S(1)} %pad_maximum_fusion.4.refs_8_), channel_id=1, source_target_pairs={{0,2},{1,3},{2,0},{3,1},{4,6},{5,7},{6,4},{7,5},{8,10},{9,11},{10,... | collective-permute-start | bytes 393224 | tf_op jit(solution)/shard_map/ppermute | solution.py:30
  133.7 7.3 %collective-permute-start.49 = (bf16[4,128,128]{2,1,0:T(8,128)(2,1)S(1)}, bf16[4,128,128]{2,1,0:T(8,128)(2,1)S(1)}, u32[]{:S(2)}, u32[]{:S(2)}) collective-permute-start(bf16[4,128,128]{2,1,0:T(8,128)(2,1)S(1)} %pad_maximum_fusion.4.refs_8_), channel_id=1, source_target_pairs={{0,6},{1,7},{2,4},{3,5},{4,2},{5,3},{6,0},{7,1},{8,14},{9,15},{10,... | collective-permute-start | bytes 393224 | tf_op jit(solution)/shard_map/ppermute | solution.py:30
  148.6 10.2 %collective-permute-start.58 = (bf16[4,256,128]{2,1,0:T(8,128)(2,1)S(1)}, bf16[4,256,128]{2,1,0:T(8,128)(2,1)S(1)}, u32[]{:S(2)}, u32[]{:S(2)}) collective-permute-start(bf16[4,256,128]{2,1,0:T(8,128)(2,1)S(1)} %add_convert_fusion.2), channel_id=1, source_target_pairs={{0,6},{1,7},{2,4},{3,5},{4,2},{5,3},{6,0},{7,1},{8,14},{9,15},{10,... | collective-permute-start | bytes 786440 | tf_op jit(solution)/shard_map/ppermute | solution.py:30
  151.3 12.4 %collective-permute-start.60 = (bf16[4,256,128]{2,1,0:T(8,128)(2,1)S(1)}, bf16[4,256,128]{2,1,0:T(8,128)(2,1)S(1)}, u32[]{:S(2)}, u32[]{:S(2)}) collective-permute-start(bf16[4,256,128]{2,1,0:T(8,128)(2,1)S(1)} %add_convert_fusion.1), channel_id=1, source_target_pairs={{0,4},{1,5},{2,6},{3,7},{4,0},{5,1},{6,2},{7,3},{8,12},{9,13},{10,... | collective-permute-start | bytes 786440 | tf_op jit(solution)/shard_map/ppermute | solution.py:30
  151.9 11.8 %collective-permute-start.62 = (bf16[4,256,128]{2,1,0:T(8,128)(2,1)S(1)}, bf16[4,256,128]{2,1,0:T(8,128)(2,1)S(1)}, u32[]{:S(2)}, u32[]{:S(2)}) collective-permute-start(bf16[4,256,128]{2,1,0:T(8,128)(2,1)S(1)} %add_convert_fusion), channel_id=1, source_target_pairs={{0,2},{1,3},{2,0},{3,1},{4,6},{5,7},{6,4},{7,5},{8,10},{9,11},{10,... | collective-permute-start | bytes 786440 | tf_op jit(solution)/shard_map/ppermute | solution.py:30
  163.9 11.1 %collective-permute-start.63 = (bf16[256,128]{1,0:T(8,128)(2,1)S(1)}, bf16[256,128]{1,0:T(8,128)(2,1)S(1)}, u32[]{:S(2)}, u32[]{:S(2)}) collective-permute-start(bf16[256,128]{1,0:T(8,128)(2,1)S(1)} %get-tuple-element.58), channel_id=1, source_target_pairs={{0,8},{1,9},{2,10},{3,11},{4,12},{5,13},{6,14},{7,15},{8,0},{9,1},... | collective-permute-start | bytes 196616 | tf_op jit(solution)/shard_map/ppermute | solution.py:30
  164.1 10.8 %collective-permute-start.65 = (bf16[256,128]{1,0:T(8,128)(2,1)S(1)}, bf16[256,128]{1,0:T(8,128)(2,1)S(1)}, u32[]{:S(2)}, u32[]{:S(2)}) collective-permute-start(bf16[256,128]{1,0:T(8,128)(2,1)S(1)} %get-tuple-element.59), channel_id=1, source_target_pairs={{0,24},{1,25},{2,26},{3,27},{4,28},{5,29},{6,30},{7,31},{8,16},{9,... | collective-permute-start | bytes 196616 | tf_op jit(solution)/shard_map/ppermute | solution.py:30
  166.2 8.7 %collective-permute-start.64 = (bf16[256,128]{1,0:T(8,128)(2,1)S(1)}, bf16[256,128]{1,0:T(8,128)(2,1)S(1)}, u32[]{:S(2)}, u32[]{:S(2)}) collective-permute-start(bf16[256,128]{1,0:T(8,128)(2,1)S(1)} %get-tuple-element.60), channel_id=1, source_target_pairs={{0,16},{1,17},{2,18},{3,19},{4,20},{5,21},{6,22},{7,23},{8,24},{9,... | collective-permute-start | bytes 196616 | tf_op jit(solution)/shard_map/ppermute | solution.py:30
  (64 other events, 722.3 us)

commit v3 on v2

--- a/solution.py
+++ b/solution.py
@@ -129,14 +129,18 @@
     *groups, owns = [stripes(group, 1, count) for group in groups]
     totals = []
     for index, own in enumerate(owns):
+        if totals:
+            own, totals[-1] = lax.optimization_barrier((own, totals[-1]))
         for mask, group in zip((NEAR_X | NEAR_Y, NEAR_Y, NEAR_X), groups):
             moved = flip(group[index].astype(bfloat16), mask)
             own = own + moved.astype(float32)
+        totals.append(own)
+    for index, own in enumerate(totals):
         total = own[0]
         for z in range(1, own.shape[0]):
             moved = flip(own[z].astype(bfloat16), NEAR_Z * z)
             total = total + moved.astype(float32)
-        totals.append(total)
+        totals[index] = total
     return jnp.concatenate(totals)
 
 
@@ -246,13 +250,9 @@
             new = jnp.sum(query[:, lanes] * written[:, lanes], axis=1, keepdims=True)
             part = new * value[:, lanes]
             for n in range(rows):
-                state = past_ref[step * rows + n, h]
-                high = state.astype(bfloat16)
-                low = (state - high.astype(float32)).astype(bfloat16)
-                terms = jnp.dot(both, high, preferred_element_type=float32)
-                terms = terms[:rows] + terms[rows:]
-                terms = terms + jnp.dot(coarse, low, preferred_element_type=float32)
-                part = part + jnp.where(row == n, terms, 0.0)
+                state = past_ref[step * rows + n, h].astype(bfloat16)
+                terms = jnp.dot(both, state, preferred_element_type=float32)
+                part = part + jnp.where(row == n, terms[:rows] + terms[rows:], 0.0)
             power = jnp.mean(part * part, axis=1, keepdims=True)
             part = part * lax.rsqrt(power + epsilon) * gain_ref[...]
             mixed[here, lanes] = part * gate[:, lanes]
@@ -276,42 +276,67 @@
     )(sums, forget_floor.reshape(1, inner), head_gain.reshape(1, size), past_state)
 
 
-def update_body(depth, sums_ref, floor_ref, past_ref, new_ref):
+def split(values, count):
+    terms = []
+    for _ in range(count):
+        terms.append(values.astype(bfloat16).astype(float32))
+        values = values - terms[-1]
+    return terms
+
+
+def update_body(depth, first, sums_ref, floor_ref, past_ref, *refs):
+    new_ref = refs[-1]
     rows, heads, size, _ = past_ref.shape
-    here = pl.ds(pl.multiple_of(pl.program_id(0) * rows, rows), rows)
+    step = first + pl.program_id(0)
+    here = pl.ds(pl.multiple_of(step * rows, rows), rows)
     _, kept, written, value, _ = gates(sums_ref, here, floor_ref[...], depth)
+    row = lax.broadcasted_iota(jnp.int32, (rows, size), 0)
+    none = jnp.zeros((rows, size), float32)
     for h in range(heads):
         lanes = slice(h * size, (h + 1) * size)
-        kept_t, written_t = kept[:, lanes].T, written[:, lanes].T
+        wide, thin = split(written[:, lanes], 2)
+        coarse, fine = split(value[:, lanes], 2)
+        columns = jnp.concatenate([wide, wide, thin] + split(kept[:, lanes], 3))
+        columns = columns.T.astype(bfloat16)
         for n in range(rows):
-            column = slice(n, n + 1)
-            new_ref[n, h] = (
-                kept_t[:, column] * past_ref[n, h]
-                + written_t[:, column] * value[column, lanes]
+            mine = row == n
+            one = jnp.where(mine, 1.0, none)
+            first_half = [jnp.where(mine, part, none) for part in (coarse, fine, coarse)]
+            spread = jnp.concatenate(
+                [
+                    jnp.concatenate(first_half + [none] * 3),
+                    jnp.concatenate([none] * 3 + [one] * 3),
+                ],
+                axis=1,
             )
-
-
-def update(sums, forget_floor, past_state, depth):
-    own_rows, heads, size, _ = past_state.shape
-    rows = min(8, own_rows)
+            both = jnp.dot(columns, spread.astype(bfloat16), preferred_element_type=float32)
+            new_ref[n, h] = both[:, size:] * past_ref[n, h] + both[:, :size]
+
+
+def update(sums, forget_floor, past_state, depth, first, count, done=None):
+    _, heads, size, _ = past_state.shape
+    rows = 8
     inner = heads * size
-    state = pl.BlockSpec((rows, heads, size, size), lambda i: (i, 0, 0, 0))
+    state = pl.BlockSpec((rows, heads, size, size), lambda i: (first + i, 0, 0, 0))
+    given = [] if done is None else [done]
     return pl.pallas_call(
-        functools.partial(update_body, depth),
-        grid=(own_rows // rows,),
+        functools.partial(update_body, depth, first),
+        grid=(count,),
         out_shape=jax.ShapeDtypeStruct(past_state.shape, float32),
         in_specs=[
             pl.BlockSpec(sums.shape, lambda i: (0, 0)),
             pl.BlockSpec((1, inner), lambda i: (0, 0)),
             state,
-        ],
+        ]
+        + [pl.BlockSpec(memory_space=pl.ANY)] * len(given),
         out_specs=state,
+        input_output_aliases={3: 0} if given else {},
         compiler_params=params(16),
         cost_estimate=pl.CostEstimate(
-            flops=2 * 10**9, bytes_accessed=8 * past_state.size, transcendentals=0
+            flops=10**9, bytes_accessed=4 * past_state.size, transcendentals=0
         ),
         name="update",
-    )(sums, forget_floor.reshape(1, inner), past_state)
+    )(sums, forget_floor.reshape(1, inner), past_state, *given)
 
 
 def gather_rows(own):
@@ -378,13 +403,18 @@
     weights = (pre_gate.T, pre_up.T, pre_down)
     seen = visit(*weights)
     partials = half_partials(me, pieces, pre_gain, *weights, seen)
-    first = (tokens.astype(float32) + 0.5 * scatter_sum(partials)).astype(bfloat16)
+    first = (tokens.astype(float32) + 0.5 * scatter_sum(partials, 2)).astype(bfloat16)
     blocks = [first] + [flip(first, mask) for mask in (CORE, NEAR_X, NEAR_X | CORE)]
     weights = (query_weight, forget_weight, value_weight, output_gate_weight)
     own_rows = past_state.shape[0]
     sums = scatter_rows(*project(me, blocks, mix_gain, weights, own_rows))
     mixed_in = read(sums, forget_floor, head_gain, past_state, depth)
-    new_state = update(sums, forget_floor, past_state, depth)
+    blocks = own_rows // 8
+    early = blocks // 2
+    new_state = update(sums, forget_floor, past_state, depth, 0, early)
+    new_state = update(
+        sums, forget_floor, past_state, depth, early, blocks - early, new_state
+    )
     parts = mix(me, gather_rows(mixed_in), proj_out)
     mixed = parts[0].astype(float32)
     for mask in (NEAR_X, NEAR_X | CORE, CORE):
@@ -393,7 +423,7 @@
     pieces = gather_all(second, 2)
     weights = (post_gate.T, post_up.T, post_down)
     partials = half_partials(me, pieces, post_gain, *weights)
-    result = (second.astype(float32) + 0.5 * scatter_sum(partials)).astype(bfloat16)
+    result = (second.astype(float32) + 0.5 * scatter_sum(partials, 2)).astype(bfloat16)
     return (result, new_state)
 
 
@@ -545,7 +575,8 @@
     def local(*arrays):
         width = arrays[0].shape[1]
         fits = mesh.shape["tp"] == 4 and mesh.shape["kv"] in (4, 8, 16)
-        plan = exchanged if fits and width == LANES else per_device
+        fits = fits and width == LANES and arrays[1].shape[0] % 16 == 0
+        plan = exchanged if fits else per_device
         return plan(*arrays)
 
     return jax.shard_map(

time: 176 us -> 178 us (1.011)
  starting transfers between devices: 63.4 us -> 74.2 us
  waiting for transfers between devices: 77.9 us -> 71.6 us
  Pallas kernels: 21.2 us -> 18.9 us
    ppermute x66 -> x78, starting transfers between devices: 63.4 us -> 74.2 us  [flip(): return lax.ppermute(block, AXES, pairs)]
    ppermute x66 -> x78, waiting for transfers between devices: 77.9 us -> 71.6 us  [flip(): return lax.ppermute(block, AXES, pairs)]
    pallas_call x1 -> x2, Pallas kernels: 7.54 us -> 6.28 us  [update(): pl.pallas_call(functools.partial(update_body, depth, first), grid=(count,...]
  transfers between devices with their start and end apart: 66 -> 78, of which waited for: 33 -> 37; matrix products, arithmetic and copies ran while one was open for 0% -> 1% of each run, Pallas kernels for 4% -> 4%
where the time goes in v3:
time: 178 us
  starting transfers between devices  74.2 us (42%)
  waiting for transfers between devices  71.6 us (40%)
  Pallas kernels  18.9 us (11%)
  local copies, waits for them, and re-layouts  9.37 us (5%)
  other arithmetic  2.73 us (2%)
    ppermute x78, starting transfers between devices, flip(): return lax.ppermute(block, AXES, pairs)  74.2 us
    ppermute x78, waiting for transfers between devices, flip(): return lax.ppermute(block, AXES, pairs)  71.6 us
    unnamed x46, local copies, waits for them, and re-layouts  9.06 us
    pallas_call x2, Pallas kernels, half_partials(): pl.pallas_call(functools.partial(half_body, masks), out_shape=[jax.ShapeD...  8.62 us
    pallas_call x2, Pallas kernels, update(): pl.pallas_call(functools.partial(update_body, depth, first), grid=(count,...  6.28 us
  transfers between devices with their start and end apart: 78, of which 37 were waited for; matrix products, arithmetic and copies ran while one was open for 1% of the time, Pallas kernels for 4%

profile of v3, /device:TPU:0, one launch (start us, length us, event | category | flops | bytes accessed | tf_op | source)
XLA Modules:
  0.0 178.2 jit_solution(16788035054943248983)
XLA Ops:
  0.6 5.1 %collective-permute-start.2 = (bf16[256,128]{1,0:T(8,128)(2,1)}, bf16[256,128]{1,0:T(8,128)(2,1)S(1)}, u32[]{:S(2)}, u32[]{:S(2)}) collective-permute-start(bf16[256,128]{1,0:T(8,128)(2,1)} %param.18), channel_id=1, source_target_pairs={{0,24},{1,25},{2,26},{3,27},{4,28},{5,29},{6,30},{7,31},{8,16},{9,... | collective-permute-start | bytes 196616 | tf_op jit(solution)/shard_map/ppermute | solution.py:30
  6.4 2.2 %collective-permute-done.2 = bf16[256,128]{1,0:T(8,128)(2,1)S(1)} collective-permute-done((bf16[256,128]{1,0:T(8,128)(2,1)}, bf16[256,128]{1,0:T(8,128)(2,1)S(1)}, u32[]{:S(2)}, u32[]{:S(2)}) %collective-permute-start.2) | collective-permute-done | bytes 65568 | tf_op jit(solution)/shard_map/ppermute | solution.py:30
  8.6 3.0 %collective-permute-done.1 = bf16[256,128]{1,0:T(8,128)(2,1)S(1)} collective-permute-done((bf16[256,128]{1,0:T(8,128)(2,1)}, bf16[256,128]{1,0:T(8,128)(2,1)S(1)}, u32[]{:S(2)}, u32[]{:S(2)}) %collective-permute-start.1) | collective-permute-done | bytes 65568 | tf_op jit(solution)/shard_map/ppermute | solution.py:30
  16.0 5.7 %collective-permute-done.5.refs_3_ = bf16[4,256,128]{2,1,0:T(8,128)(2,1)S(1)} collective-permute-done((bf16[4,256,128]{2,1,0:T(8,128)(2,1)S(1)}, bf16[4,256,128]{2,1,0:T(8,128)(2,1)S(1)}, u32[]{:S(2)}, u32[]{:S(2)}) %collective-permute-start.5) | collective-permute-done | bytes 262176 | tf_op jit(solution)/shard_map/ppermute | solution.py:30
  21.7 5.6 %collective-permute-done.4.refs_2_ = bf16[4,256,128]{2,1,0:T(8,128)(2,1)S(1)} collective-permute-done((bf16[4,256,128]{2,1,0:T(8,128)(2,1)S(1)}, bf16[4,256,128]{2,1,0:T(8,128)(2,1)S(1)}, u32[]{:S(2)}, u32[]{:S(2)}) %collective-permute-start.4) | collective-permute-done | bytes 262176 | tf_op jit(solution)/shard_map/ppermute | solution.py:30
  36.9 4.4 %half_step.2 = (bf16[4,256,128]{2,1,0:T(8,128)(2,1)S(1)}, bf16[4,256,128]{2,1,0:T(8,128)(2,1)S(1)}, bf16[4,256,128]{2,1,0:T(8,128)(2,1)S(1)}, bf16[4,256,128]{2,...) custom-call(s32[1]{0:T(128)} %bitcast.me_ref, ...), custom_call_target="tpu_custom_call" | custom-call | tf_op jit(solution)/shard_map/half_step/pallas_call | solution.py:113
  49.2 3.9 %collective-permute-done.12 = bf16[4,128,128]{2,1,0:T(8,128)(2,1)S(1)} collective-permute-done((bf16[4,128,128]{2,1,0:T(8,128)(2,1)S(1)}, bf16[4,128,128]{2,1,0:T(8,128)(2,1)S(1)}, u32[]{:S(2)}, u32[]{:S(2)}) %collective-permute-start.12) | collective-permute-done | bytes 131104 | tf_op jit(solution)/shard_map/ppermute | solution.py:30
  64.2 2.3 %collective-permute-done.25 = bf16[128,128]{1,0:T(8,128)(2,1)S(1)} collective-permute-done((bf16[128,128]{1,0:T(8,128)(2,1)S(1)}, bf16[128,128]{1,0:T(8,128)(2,1)S(1)}, u32[]{:S(2)}, u32[]{:S(2)}) %collective-permute-start.25) | collective-permute-done | bytes 32800 | tf_op jit(solution)/shard_map/ppermute | solution.py:30
  74.5 7.3 %collective-permute-done.32 = bf16[2,2,32,1024]{3,2,0,1:T(8,128)(2,1)S(1)} collective-permute-done((bf16[2,2,32,1024]{3,2,0,1:T(8,128)(2,1)S(1)}, bf16[2,2,32,1024]{3,2,0,1:T(8,128)(2,1)S(1)}, u32[]{:S(2)}, u32[]{:S(2)}) %collective-permute-start.32) | collective-permute-done | bytes 262176 | tf_op jit(solution)/shard_map/ppermute | solution.py:30
  84.8 2.1 %collective-permute-done.33 = bf16[2,32,1024]{2,1,0:T(8,128)(2,1)S(1)} collective-permute-done((bf16[2,32,1024]{2,1,0:T(8,128)(2,1)S(1)}, bf16[2,32,1024]{2,1,0:T(8,128)(2,1)S(1)}, u32[]{:S(2)}, u32[]{:S(2)}) %collective-permute-start.33) | collective-permute-done | bytes 131104 | tf_op jit(solution)/shard_map/ppermute | solution.py:30
  88.1 3.4 %collective-permute-start.31 = (bf16[32,1152]{1,0:T(8,128)(2,1)S(1)}, bf16[32,1152]{1,0:T(8,128)(2,1)S(1)}, u32[]{:S(2)}, u32[]{:S(2)}) collective-permute-start(bf16[32,1152]{1,0:T(8,128)(2,1)S(1)} %fusion.14), channel_id=1, source_target_pairs={{0,16},{1,17},{2,18},{3,19},{4,20},{5,21},{6,22},{7,23},{8,24},{9,... | collective-permute-start | bytes 221192 | tf_op jit(solution)/shard_map/ppermute | solution.py:30
  94.2 2.7 %read.1 = bf16[32,512]{1,0:T(8,128)(2,1)S(1)} custom-call(f32[32,2176]{1,0:T(8,128)S(1)} %pad_maximum_fusion.sums_ref, f32[1,512]{1,0:T(1,128)S(1)} %bitcast.133, f32[1,128]{1,0:T(1,128)S(1)} %bitcast.139, f32[32,4,128,128]{3,2,1,0:T(8,128)S(1)} %bitcast.123), custom_call_target="tpu_custom_call" | custom-call | tf_op jit(solution)/shard_map/read/pallas_call | solution.py:268
  96.9 2.1 %collective-permute-start.37 = (bf16[32,512]{1,0:T(8,128)(2,1)S(1)}, bf16[32,512]{1,0:T(8,128)(2,1)S(1)}, u32[]{:S(2)}, u32[]{:S(2)}) collective-permute-start(bf16[32,512]{1,0:T(8,128)(2,1)S(1)} %read.1), channel_id=1, source_target_pairs={{0,24},{1,25},{2,26},{3,27},{4,28},{5,29},{6,30},{7,31},{8,16},{9,... | collective-permute-start | bytes 98312 | tf_op jit(solution)/shard_map/ppermute | solution.py:30
  105.2 4.1 %collective-permute-done.38.far = bf16[4,32,512]{2,1,0:T(8,128)(2,1)S(1)} collective-permute-done((bf16[4,32,512]{2,1,0:T(8,128)(2,1)S(1)}, bf16[4,32,512]{2,1,0:T(8,128)(2,1)S(1)}, u32[]{:S(2)}, u32[]{:S(2)}) %collective-permute-start.38) | collective-permute-done | bytes 131104 | tf_op jit(solution)/shard_map/ppermute | solution.py:30
  111.9 2.4 %collective-permute-done.39 = bf16[256,128]{1,0:T(8,128)(2,1)S(1)} collective-permute-done((bf16[256,128]{1,0:T(8,128)(2,1)S(1)}, bf16[256,128]{1,0:T(8,128)(2,1)S(1)}, u32[]{:S(2)}, u32[]{:S(2)}) %collective-permute-start.39) | collective-permute-done | bytes 65568 | tf_op jit(solution)/shard_map/ppermute | solution.py:30
  120.5 2.1 %collective-permute-start.52 = (bf16[128,128]{1,0:T(8,128)(2,1)S(1)}, bf16[128,128]{1,0:T(8,128)(2,1)S(1)}, u32[]{:S(2)}, u32[]{:S(2)}) collective-permute-start(bf16[128,128]{1,0:T(8,128)(2,1)S(1)} %get-tuple-element.96), channel_id=1, source_target_pairs={{0,8},{1,9},{2,10},{3,11},{4,12},{5,13},{6,14},{7,15},{8,0},{9,1},... | collective-permute-start | bytes 98312 | tf_op jit(solution)/shard_map/ppermute | solution.py:30
  131.7 2.4 %collective-permute-done.46.refs_2_ = bf16[4,128,128]{2,1,0:T(8,128)(2,1)S(1)} collective-permute-done((bf16[4,128,128]{2,1,0:T(8,128)(2,1)S(1)}, bf16[4,128,128]{2,1,0:T(8,128)(2,1)S(1)}, u32[]{:S(2)}, u32[]{:S(2)}) %collective-permute-start.46) | collective-permute-done | bytes 131104 | tf_op jit(solution)/shard_map/ppermute | solution.py:30
  141.6 4.3 %half_step.3 = (bf16[4,256,128]{2,1,0:T(8,128)(2,1)S(1)}, bf16[4,256,128]{2,1,0:T(8,128)(2,1)S(1)}, bf16[4,256,128]{2,1,0:T(8,128)(2,1)S(1)}, bf16[4,256,128]{2,...) custom-call(s32[1]{0:T(128)} %bitcast.me_ref, ...), custom_call_target="tpu_custom_call" | custom-call | tf_op jit(solution)/shard_map/half_step/pallas_call | solution.py:113
  146.3 3.1 %update.2.refs_0_ = f32[32,4,128,128]{3,2,1,0:T(8,128)} custom-call(f32[32,2176]{1,0:T(8,128)S(1)} %pad_maximum_fusion.sums_ref, f32[1,512]{1,0:T(1,128)S(1)} %bitcast.134, f32[32,4,128,128]{3,2,1,0:T(8,128)S(1)} %bitcast.123), custom_call_target="tpu_custom_call" | custom-call | flops 1000000000 | bytes 8388608 | tf_op jit(solution)/shard_map/update/pallas_call | solution.py:322
  149.4 3.1 %update.3 = f32[32,4,128,128]{3,2,1,0:T(8,128)} custom-call(f32[32,2176]{1,0:T(8,128)S(1)} %pad_maximum_fusion.sums_ref, f32[1,512]{1,0:T(1,128)S(1)} %bitcast.135, f32[32,4,128,128]{3,2,1,0:T(8,128)S(1)} %bitcast.123, f32[32,4,128,128]{3,2,1,0:T(8,128)} %update.2.refs_0_), custom_call_target="tpu_custom_call", output_to_operand_aliasing={{}: (3, {})} | custom-call | flops 1000000000 | bytes 8388608 | tf_op jit(solution)/shard_map/update/pallas_call | solution.py:322
  159.6 4.0 %collective-permute-done.64 = bf16[4,128,128]{2,1,0:T(8,128)(2,1)S(1)} collective-permute-done((bf16[4,128,128]{2,1,0:T(8,128)(2,1)S(1)}, bf16[4,128,128]{2,1,0:T(8,128)(2,1)S(1)}, u32[]{:S(2)}, u32[]{:S(2)}) %collective-permute-start.64) | collective-permute-done | bytes 131104 | tf_op jit(solution)/shard_map/ppermute | solution.py:30
  165.9 2.2 %collective-permute-start.71 = (bf16[128,128]{1,0:T(8,128)(2,1)S(1)}, bf16[128,128]{1,0:T(8,128)(2,1)S(1)}, u32[]{:S(2)}, u32[]{:S(2)}) collective-permute-start(bf16[128,128]{1,0:T(8,128)(2,1)S(1)} %get-tuple-element.83), channel_id=1, source_target_pairs={{0,24},{1,25},{2,26},{3,27},{4,28},{5,29},{6,30},{7,31},{8,16},{9,... | collective-permute-start | bytes 98312 | tf_op jit(solution)/shard_map/ppermute | solution.py:30
  170.6 2.1 %collective-permute-start.77 = (bf16[128,128]{1,0:T(8,128)(2,1)S(1)}, bf16[128,128]{1,0:T(8,128)(2,1)S(1)}, u32[]{:S(2)}, u32[]{:S(2)}) collective-permute-start(bf16[128,128]{1,0:T(8,128)(2,1)S(1)} %get-tuple-element.86), channel_id=1, source_target_pairs={{0,24},{1,25},{2,26},{3,27},{4,28},{5,29},{6,30},{7,31},{8,16},{9,... | collective-permute-start | bytes 98312 | tf_op jit(solution)/shard_map/ppermute | solution.py:30
  173.5 2.8 %collective-permute-done.77 = bf16[128,128]{1,0:T(8,128)(2,1)S(1)} collective-permute-done((bf16[128,128]{1,0:T(8,128)(2,1)S(1)}, bf16[128,128]{1,0:T(8,128)(2,1)S(1)}, u32[]{:S(2)}, u32[]{:S(2)}) %collective-permute-start.77) | collective-permute-done | bytes 32800 | tf_op jit(solution)/shard_map/ppermute | solution.py:30
  (236 shorter events, 94.4 us)
Async XLA Ops:
  0.6 7.9 %collective-permute-start.2 = (bf16[256,128]{1,0:T(8,128)(2,1)}, bf16[256,128]{1,0:T(8,128)(2,1)S(1)}, u32[]{:S(2)}, u32[]{:S(2)}) collective-permute-start(bf16[256,128]{1,0:T(8,128)(2,1)} %param.18), channel_id=1, source_target_pairs={{0,24},{1,25},{2,26},{3,27},{4,28},{5,29},{6,30},{7,31},{8,16},{9,... | collective-permute-start | bytes 196616 | tf_op jit(solution)/shard_map/ppermute | solution.py:30
  12.5 9.2 %collective-permute-start.5 = (bf16[4,256,128]{2,1,0:T(8,128)(2,1)S(1)}, bf16[4,256,128]{2,1,0:T(8,128)(2,1)S(1)}, u32[]{:S(2)}, u32[]{:S(2)}) collective-permute-start(bf16[4,256,128]{2,1,0:T(8,128)(2,1)S(1)} %pad_maximum_fusion.1.refs_0_), channel_id=1, source_target_pairs={{0,2},{1,3},{2,0},{3,1},{4,6},{5,7},{6,4},{7,5},{8,10},{9,11},{10,... | collective-permute-start | bytes 786440 | tf_op jit(solution)/shard_map/ppermute | solution.py:30
  14.0 13.3 %collective-permute-start.4 = (bf16[4,256,128]{2,1,0:T(8,128)(2,1)S(1)}, bf16[4,256,128]{2,1,0:T(8,128)(2,1)S(1)}, u32[]{:S(2)}, u32[]{:S(2)}) collective-permute-start(bf16[4,256,128]{2,1,0:T(8,128)(2,1)S(1)} %pad_maximum_fusion.1.refs_0_), channel_id=1, source_target_pairs={{0,4},{1,5},{2,6},{3,7},{4,0},{5,1},{6,2},{7,3},{8,12},{9,13},{10,... | collective-permute-start | bytes 786440 | tf_op jit(solution)/shard_map/ppermute | solution.py:30
  15.6 11.8 %collective-permute-start.3 = (bf16[4,256,128]{2,1,0:T(8,128)(2,1)S(1)}, bf16[4,256,128]{2,1,0:T(8,128)(2,1)S(1)}, u32[]{:S(2)}, u32[]{:S(2)}) collective-permute-start(bf16[4,256,128]{2,1,0:T(8,128)(2,1)S(1)} %pad_maximum_fusion.1.refs_0_), channel_id=1, source_target_pairs={{0,6},{1,7},{2,4},{3,5},{4,2},{5,3},{6,0},{7,1},{8,14},{9,15},{10,... | collective-permute-start | bytes 786440 | tf_op jit(solution)/shard_map/ppermute | solution.py:30
  16.0 17.3 %collective-permute-start.6 = (bf16[4,256,128]{2,1,0:T(8,128)(2,1)S(1)}, bf16[4,256,128]{2,1,0:T(8,128)(2,1)S(1)}, u32[]{:S(2)}, u32[]{:S(2)}) collective-permute-start(bf16[4,256,128]{2,1,0:T(8,128)(2,1)S(1)} %pad_maximum_fusion.1.refs_0_), channel_id=1, source_target_pairs={{0,1},{1,0},{2,3},{3,2},{4,5},{5,4},{6,7},{7,6},{8,9},{9,8},{10,11... | collective-permute-start | bytes 786440 | tf_op jit(solution)/shard_map/ppermute | solution.py:30
  21.7 11.6 %collective-permute-start.9 = (bf16[4,256,128]{2,1,0:T(8,128)(2,1)S(1)}, bf16[4,256,128]{2,1,0:T(8,128)(2,1)S(1)}, u32[]{:S(2)}, u32[]{:S(2)}) collective-permute-start(bf16[4,256,128]{2,1,0:T(8,128)(2,1)S(1)} %collective-permute-done.5.refs_3_), channel_id=1, source_target_pairs={{0,1},{1,0},{2,3},{3,2},{4,5},{5,4},{6,7},{7,6},{8,9},{9,8},{10,11... | collective-permute-start | bytes 786440 | tf_op jit(solution)/shard_map/ppermute | solution.py:30
  42.9 14.9 %collective-permute-start.20 = (bf16[4,128,128]{2,1,0:T(8,128)(2,1)S(1)}, bf16[4,128,128]{2,1,0:T(8,128)(2,1)S(1)}, u32[]{:S(2)}, u32[]{:S(2)}) collective-permute-start(bf16[4,128,128]{2,1,0:T(8,128)(2,1)S(1)} %get-tuple-element.76), channel_id=1, source_target_pairs={{0,6},{1,7},{2,4},{3,5},{4,2},{5,3},{6,0},{7,1},{8,14},{9,15},{10,... | collective-permute-start | bytes 393224 | tf_op jit(solution)/shard_map/ppermute | solution.py:30
  44.5 8.6 %collective-permute-start.12 = (bf16[4,128,128]{2,1,0:T(8,128)(2,1)S(1)}, bf16[4,128,128]{2,1,0:T(8,128)(2,1)S(1)}, u32[]{:S(2)}, u32[]{:S(2)}) collective-permute-start(bf16[4,128,128]{2,1,0:T(8,128)(2,1)S(1)} %get-tuple-element.77), channel_id=1, source_target_pairs={{0,6},{1,7},{2,4},{3,5},{4,2},{5,3},{6,0},{7,1},{8,14},{9,15},{10,... | collective-permute-start | bytes 393224 | tf_op jit(solution)/shard_map/ppermute | solution.py:30
  46.0 9.1 %collective-permute-start.14 = (bf16[4,128,128]{2,1,0:T(8,128)(2,1)S(1)}, bf16[4,128,128]{2,1,0:T(8,128)(2,1)S(1)}, u32[]{:S(2)}, u32[]{:S(2)}) collective-permute-start(bf16[4,128,128]{2,1,0:T(8,128)(2,1)S(1)} %get-tuple-element.78), channel_id=1, source_target_pairs={{0,4},{1,5},{2,6},{3,7},{4,0},{5,1},{6,2},{7,3},{8,12},{9,13},{10,... | collective-permute-start | bytes 393224 | tf_op jit(solution)/shard_map/ppermute | solution.py:30
  47.6 12.1 %collective-permute-start.21 = (bf16[4,128,128]{2,1,0:T(8,128)(2,1)S(1)}, bf16[4,128,128]{2,1,0:T(8,128)(2,1)S(1)}, u32[]{:S(2)}, u32[]{:S(2)}) collective-permute-start(bf16[4,128,128]{2,1,0:T(8,128)(2,1)S(1)} %get-tuple-element.79), channel_id=1, source_target_pairs={{0,4},{1,5},{2,6},{3,7},{4,0},{5,1},{6,2},{7,3},{8,12},{9,13},{10,... | collective-permute-start | bytes 393224 | tf_op jit(solution)/shard_map/ppermute | solution.py:30
  48.3 7.7 %collective-permute-start.16 = (bf16[4,128,128]{2,1,0:T(8,128)(2,1)S(1)}, bf16[4,128,128]{2,1,0:T(8,128)(2,1)S(1)}, u32[]{:S(2)}, u32[]{:S(2)}) collective-permute-start(bf16[4,128,128]{2,1,0:T(8,128)(2,1)S(1)} %get-tuple-element.80), channel_id=1, source_target_pairs={{0,2},{1,3},{2,0},{3,1},{4,6},{5,7},{6,4},{7,5},{8,10},{9,11},{10,... | collective-permute-start | bytes 393224 | tf_op jit(solution)/shard_map/ppermute | solution.py:30
  56.2 7.1 %collective-permute-start.19 = (bf16[128,128]{1,0:T(8,128)(2,1)S(1)}, bf16[128,128]{1,0:T(8,128)(2,1)S(1)}, u32[]{:S(2)}, u32[]{:S(2)}) collective-permute-start(bf16[128,128]{1,0:T(8,128)(2,1)S(1)} %get-tuple-element.89), channel_id=1, source_target_pairs={{0,24},{1,25},{2,26},{3,27},{4,28},{5,29},{6,30},{7,31},{8,16},{9,... | collective-permute-start | bytes 98312 | tf_op jit(solution)/shard_map/ppermute | solution.py:30
  73.4 8.4 %collective-permute-start.32 = (bf16[2,2,32,1024]{3,2,0,1:T(8,128)(2,1)S(1)}, bf16[2,2,32,1024]{3,2,0,1:T(8,128)(2,1)S(1)}, u32[]{:S(2)}, u32[]{:S(2)}) collective-permute-start(bf16[2,2,32,1024]{3,2,0,1:T(8,128)(2,1)S(1)} %bitcast.141), channel_id=1, source_target_pairs={{0,8},{1,9},{2,10},{3,11},{4,12},{5,13},{6,14},{7,15},{8,0},{9,1},... | collective-permute-start | bytes 786440 | tf_op jit(solution)/shard_map/ppermute | solution.py:30
  73.8 8.9 %collective-permute-start.29 = (bf16[2,2,32,1152]{3,2,0,1:T(8,128)(2,1)S(1)}, bf16[2,2,32,1152]{3,2,0,1:T(8,128)(2,1)S(1)}, u32[]{:S(2)}, u32[]{:S(2)}) collective-permute-start(bf16[2,2,32,1152]{3,2,0,1:T(8,128)(2,1)S(1)} %bitcast.140), channel_id=1, source_target_pairs={{0,4},{1,5},{2,6},{3,7},{4,0},{5,1},{6,2},{7,3},{8,12},{9,13},{10,... | collective-permute-start | bytes 884744 | tf_op jit(solution)/shard_map/ppermute | solution.py:30
  115.3 7.3 %collective-permute-start.43 = (bf16[128,128]{1,0:T(8,128)(2,1)S(1)}, bf16[128,128]{1,0:T(8,128)(2,1)S(1)}, u32[]{:S(2)}, u32[]{:S(2)}) collective-permute-start(bf16[128,128]{1,0:T(8,128)(2,1)S(1)} %get-tuple-element.97), channel_id=1, source_target_pairs={{0,16},{1,17},{2,18},{3,19},{4,20},{5,21},{6,22},{7,23},{8,24},{9,... | collective-permute-start | bytes 98312 | tf_op jit(solution)/shard_map/ppermute | solution.py:30
  125.5 8.7 %collective-permute-start.46 = (bf16[4,128,128]{2,1,0:T(8,128)(2,1)S(1)}, bf16[4,128,128]{2,1,0:T(8,128)(2,1)S(1)}, u32[]{:S(2)}, u32[]{:S(2)}) collective-permute-start(bf16[4,128,128]{2,1,0:T(8,128)(2,1)S(1)} %pad_maximum_fusion.3.refs_0_), channel_id=1, source_target_pairs={{0,4},{1,5},{2,6},{3,7},{4,0},{5,1},{6,2},{7,3},{8,12},{9,13},{10,... | collective-permute-start | bytes 393224 | tf_op jit(solution)/shard_map/ppermute | solution.py:30
  126.2 8.7 %collective-permute-start.45 = (bf16[4,128,128]{2,1,0:T(8,128)(2,1)S(1)}, bf16[4,128,128]{2,1,0:T(8,128)(2,1)S(1)}, u32[]{:S(2)}, u32[]{:S(2)}) collective-permute-start(bf16[4,128,128]{2,1,0:T(8,128)(2,1)S(1)} %pad_maximum_fusion.3.refs_0_), channel_id=1, source_target_pairs={{0,6},{1,7},{2,4},{3,5},{4,2},{5,3},{6,0},{7,1},{8,14},{9,15},{10,... | collective-permute-start | bytes 393224 | tf_op jit(solution)/shard_map/ppermute | solution.py:30
  128.4 7.9 %collective-permute-start.57 = (bf16[4,128,128]{2,1,0:T(8,128)(2,1)S(1)}, bf16[4,128,128]{2,1,0:T(8,128)(2,1)S(1)}, u32[]{:S(2)}, u32[]{:S(2)}) collective-permute-start(bf16[4,128,128]{2,1,0:T(8,128)(2,1)S(1)} %pad_maximum_fusion.4.refs_8_), channel_id=1, source_target_pairs={{0,2},{1,3},{2,0},{3,1},{4,6},{5,7},{6,4},{7,5},{8,10},{9,11},{10,... | collective-permute-start | bytes 393224 | tf_op jit(solution)/shard_map/ppermute | solution.py:30
  130.6 7.4 %collective-permute-start.56 = (bf16[4,128,128]{2,1,0:T(8,128)(2,1)S(1)}, bf16[4,128,128]{2,1,0:T(8,128)(2,1)S(1)}, u32[]{:S(2)}, u32[]{:S(2)}) collective-permute-start(bf16[4,128,128]{2,1,0:T(8,128)(2,1)S(1)} %pad_maximum_fusion.4.refs_8_), channel_id=1, source_target_pairs={{0,4},{1,5},{2,6},{3,7},{4,0},{5,1},{6,2},{7,3},{8,12},{9,13},{10,... | collective-permute-start | bytes 393224 | tf_op jit(solution)/shard_map/ppermute | solution.py:30
  145.9 7.4 %collective-permute-start.63 = (bf16[4,256,128]{2,1,0:T(8,128)(2,1)S(1)}, bf16[4,256,128]{2,1,0:T(8,128)(2,1)S(1)}, u32[]{:S(2)}, u32[]{:S(2)}) collective-permute-start(bf16[4,256,128]{2,1,0:T(8,128)(2,1)S(1)} %get-tuple-element.51), channel_id=1, source_target_pairs={{0,1},{1,0},{2,3},{3,2},{4,5},{5,4},{6,7},{7,6},{8,9},{9,8},{10,11... | collective-permute-start | bytes 786440 | tf_op jit(solution)/shard_map/ppermute | solution.py:30
  153.4 14.8 %collective-permute-start.72 = (bf16[4,128,128]{2,1,0:T(8,128)(2,1)S(1)}, bf16[4,128,128]{2,1,0:T(8,128)(2,1)S(1)}, u32[]{:S(2)}, u32[]{:S(2)}) collective-permute-start(bf16[4,128,128]{2,1,0:T(8,128)(2,1)S(1)} %get-tuple-element.70), channel_id=1, source_target_pairs={{0,6},{1,7},{2,4},{3,5},{4,2},{5,3},{6,0},{7,1},{8,14},{9,15},{10,... | collective-permute-start | bytes 393224 | tf_op jit(solution)/shard_map/ppermute | solution.py:30
  154.5 9.0 %collective-permute-start.64 = (bf16[4,128,128]{2,1,0:T(8,128)(2,1)S(1)}, bf16[4,128,128]{2,1,0:T(8,128)(2,1)S(1)}, u32[]{:S(2)}, u32[]{:S(2)}) collective-permute-start(bf16[4,128,128]{2,1,0:T(8,128)(2,1)S(1)} %get-tuple-element.71), channel_id=1, source_target_pairs={{0,6},{1,7},{2,4},{3,5},{4,2},{5,3},{6,0},{7,1},{8,14},{9,15},{10,... | collective-permute-start | bytes 393224 | tf_op jit(solution)/shard_map/ppermute | solution.py:30
  156.4 9.3 %collective-permute-start.66 = (bf16[4,128,128]{2,1,0:T(8,128)(2,1)S(1)}, bf16[4,128,128]{2,1,0:T(8,128)(2,1)S(1)}, u32[]{:S(2)}, u32[]{:S(2)}) collective-permute-start(bf16[4,128,128]{2,1,0:T(8,128)(2,1)S(1)} %get-tuple-element.72), channel_id=1, source_target_pairs={{0,4},{1,5},{2,6},{3,7},{4,0},{5,1},{6,2},{7,3},{8,12},{9,13},{10,... | collective-permute-start | bytes 393224 | tf_op jit(solution)/shard_map/ppermute | solution.py:30
  156.9 12.5 %collective-permute-start.73 = (bf16[4,128,128]{2,1,0:T(8,128)(2,1)S(1)}, bf16[4,128,128]{2,1,0:T(8,128)(2,1)S(1)}, u32[]{:S(2)}, u32[]{:S(2)}) collective-permute-start(bf16[4,128,128]{2,1,0:T(8,128)(2,1)S(1)} %get-tuple-element.73), channel_id=1, source_target_pairs={{0,4},{1,5},{2,6},{3,7},{4,0},{5,1},{6,2},{7,3},{8,12},{9,13},{10,... | collective-permute-start | bytes 393224 | tf_op jit(solution)/shard_map/ppermute | solution.py:30
  (76 other events, 758.6 us)

commit v4 on v3

--- a/solution.py
+++ b/solution.py
@@ -85,13 +85,13 @@
             normed[here, columns] = (block * gain_ref[:, columns]).astype(bfloat16)
             squares[row] = squares[row] + block * block if row in squares else block * block
     total = jnp.concatenate([squares[row] for row in sorted(squares)])
-    scale = lax.rsqrt(jnp.sum(total, axis=1, keepdims=True) / depth + epsilon)
+    scale = lax.rsqrt(jnp.sum(total.T, axis=0, keepdims=True) / depth + epsilon)
     across = (((1,), (1,)), ((), ()))
     gate, up = (
-        scale * lax.dot_general(normed[...], weight[...], across, preferred_element_type=float32)
+        scale * lax.dot_general(weight[...], normed[...], across, preferred_element_type=float32)
         for weight in (gate_ref, up_ref)
     )
-    hidden = (gate * jax.nn.sigmoid(gate) * up).astype(bfloat16)
+    hidden = (gate * jax.nn.sigmoid(gate) * up).T.astype(bfloat16)
     low = (me & CORE) == 0
     for group, mask in enumerate((NEAR_X | NEAR_Y, NEAR_Y, NEAR_X, 0)):
         for z in range(keeps[group].shape[0]):
@@ -241,18 +241,30 @@
         here = pl.ds(pl.multiple_of(step * rows, rows), rows)
         query, kept, written, value, gate = gates(sums_ref, here, floors, depth)
         row = lax.broadcasted_iota(jnp.int32, (rows, size), 0)
+        asks = []
         for h in range(heads):
             lanes = slice(h * size, (h + 1) * size)
             ask = query[:, lanes] * kept[:, lanes]
             coarse = ask.astype(bfloat16)
             fine = (ask - coarse.astype(float32)).astype(bfloat16)
-            both = jnp.concatenate([coarse, fine])
+            asks.append(jnp.concatenate([coarse, fine]))
+        both = jnp.concatenate(asks)
+        answers = [0.0] * heads
+        for n in range(rows):
+            for h in range(0, heads, 2):
+                state = jnp.concatenate(
+                    [past_ref[step * rows + n, h + i].astype(bfloat16) for i in range(2)], axis=1
+                )
+                pair = both[2 * rows * h : 2 * rows * (h + 2)]
+                terms = jnp.dot(pair, state, preferred_element_type=float32)
+                for i in range(2):
+                    own = terms[2 * rows * i :, i * size : (i + 1) * size]
+                    own = own[:rows] + own[rows : 2 * rows]
+                    answers[h + i] = answers[h + i] + jnp.where(row == n, own, 0.0)
+        for h in range(heads):
+            lanes = slice(h * size, (h + 1) * size)
             new = jnp.sum(query[:, lanes] * written[:, lanes], axis=1, keepdims=True)
-            part = new * value[:, lanes]
-            for n in range(rows):
-                state = past_ref[step * rows + n, h].astype(bfloat16)
-                terms = jnp.dot(both, state, preferred_element_type=float32)
-                part = part + jnp.where(row == n, terms[:rows] + terms[rows:], 0.0)
+            part = answers[h] + new * value[:, lanes]
             power = jnp.mean(part * part, axis=1, keepdims=True)
             part = part * lax.rsqrt(power + epsilon) * gain_ref[...]
             mixed[here, lanes] = part * gate[:, lanes]

time: 178 us -> 177 us (level)
  transfers between devices with their start and end apart: 78 -> 78, of which waited for: 37 -> 38; matrix products, arithmetic and copies ran while one was open for 1% -> 1% of each run, Pallas kernels for 4% -> 4%
where the time goes in v4:
time: 177 us
  starting transfers between devices  74.4 us (42%)
  waiting for transfers between devices  71.4 us (40%)
  Pallas kernels  17.4 us (10%)
  local copies, waits for them, and re-layouts  9.37 us (5%)
  other arithmetic  2.73 us (2%)
    ppermute x78, starting transfers between devices, flip(): return lax.ppermute(block, AXES, pairs)  74.4 us
    ppermute x78, waiting for transfers between devices, flip(): return lax.ppermute(block, AXES, pairs)  71.4 us
    unnamed x46, local copies, waits for them, and re-layouts  9.06 us
    pallas_call x2, Pallas kernels, half_partials(): pl.pallas_call(functools.partial(half_body, masks), out_shape=[jax.ShapeD...  7.59 us
    pallas_call x2, Pallas kernels, update(): pl.pallas_call(functools.partial(update_body, depth, first), grid=(count,...  6.29 us
  transfers between devices with their start and end apart: 78, of which 38 were waited for; matrix products, arithmetic and copies ran while one was open for 1% of the time, Pallas kernels for 4%

profile of v4, /device:TPU:0, one launch (start us, length us, event | category | flops | bytes accessed | tf_op | source)
XLA Modules:
  0.0 176.7 jit_solution(1403938839408252143)
XLA Ops:
  0.6 5.1 %collective-permute-start.2 = (bf16[256,128]{1,0:T(8,128)(2,1)}, bf16[256,128]{1,0:T(8,128)(2,1)S(1)}, u32[]{:S(2)}, u32[]{:S(2)}) collective-permute-start(bf16[256,128]{1,0:T(8,128)(2,1)} %param.18), channel_id=1, source_target_pairs={{0,24},{1,25},{2,26},{3,27},{4,28},{5,29},{6,30},{7,31},{8,16},{9,... | collective-permute-start | bytes 196616 | tf_op jit(solution)/shard_map/ppermute | solution.py:30
  6.4 2.2 %collective-permute-done.2 = bf16[256,128]{1,0:T(8,128)(2,1)S(1)} collective-permute-done((bf16[256,128]{1,0:T(8,128)(2,1)}, bf16[256,128]{1,0:T(8,128)(2,1)S(1)}, u32[]{:S(2)}, u32[]{:S(2)}) %collective-permute-start.2) | collective-permute-done | bytes 65568 | tf_op jit(solution)/shard_map/ppermute | solution.py:30
  8.6 3.0 %collective-permute-done.1 = bf16[256,128]{1,0:T(8,128)(2,1)S(1)} collective-permute-done((bf16[256,128]{1,0:T(8,128)(2,1)}, bf16[256,128]{1,0:T(8,128)(2,1)S(1)}, u32[]{:S(2)}, u32[]{:S(2)}) %collective-permute-start.1) | collective-permute-done | bytes 65568 | tf_op jit(solution)/shard_map/ppermute | solution.py:30
  16.0 5.7 %collective-permute-done.5.refs_3_ = bf16[4,256,128]{2,1,0:T(8,128)(2,1)S(1)} collective-permute-done((bf16[4,256,128]{2,1,0:T(8,128)(2,1)S(1)}, bf16[4,256,128]{2,1,0:T(8,128)(2,1)S(1)}, u32[]{:S(2)}, u32[]{:S(2)}) %collective-permute-start.5) | collective-permute-done | bytes 262176 | tf_op jit(solution)/shard_map/ppermute | solution.py:30
  21.7 5.6 %collective-permute-done.4.refs_2_ = bf16[4,256,128]{2,1,0:T(8,128)(2,1)S(1)} collective-permute-done((bf16[4,256,128]{2,1,0:T(8,128)(2,1)S(1)}, bf16[4,256,128]{2,1,0:T(8,128)(2,1)S(1)}, u32[]{:S(2)}, u32[]{:S(2)}) %collective-permute-start.4) | collective-permute-done | bytes 262176 | tf_op jit(solution)/shard_map/ppermute | solution.py:30
  36.9 3.8 %half_step.2 = (bf16[4,256,128]{2,1,0:T(8,128)(2,1)S(1)}, bf16[4,256,128]{2,1,0:T(8,128)(2,1)S(1)}, bf16[4,256,128]{2,1,0:T(8,128)(2,1)S(1)}, bf16[4,256,128]{2,...) custom-call(s32[1]{0:T(128)} %bitcast.me_ref, ...), custom_call_target="tpu_custom_call" | custom-call | tf_op jit(solution)/shard_map/half_step/pallas_call | solution.py:113
  48.7 3.8 %collective-permute-done.12 = bf16[4,128,128]{2,1,0:T(8,128)(2,1)S(1)} collective-permute-done((bf16[4,128,128]{2,1,0:T(8,128)(2,1)S(1)}, bf16[4,128,128]{2,1,0:T(8,128)(2,1)S(1)}, u32[]{:S(2)}, u32[]{:S(2)}) %collective-permute-start.12) | collective-permute-done | bytes 131104 | tf_op jit(solution)/shard_map/ppermute | solution.py:30
  63.7 2.3 %collective-permute-done.25 = bf16[128,128]{1,0:T(8,128)(2,1)S(1)} collective-permute-done((bf16[128,128]{1,0:T(8,128)(2,1)S(1)}, bf16[128,128]{1,0:T(8,128)(2,1)S(1)}, u32[]{:S(2)}, u32[]{:S(2)}) %collective-permute-start.25) | collective-permute-done | bytes 32800 | tf_op jit(solution)/shard_map/ppermute | solution.py:30
  74.0 7.3 %collective-permute-done.32 = bf16[2,2,32,1024]{3,2,0,1:T(8,128)(2,1)S(1)} collective-permute-done((bf16[2,2,32,1024]{3,2,0,1:T(8,128)(2,1)S(1)}, bf16[2,2,32,1024]{3,2,0,1:T(8,128)(2,1)S(1)}, u32[]{:S(2)}, u32[]{:S(2)}) %collective-permute-start.32) | collective-permute-done | bytes 262176 | tf_op jit(solution)/shard_map/ppermute | solution.py:30
  84.3 2.1 %collective-permute-done.33 = bf16[2,32,1024]{2,1,0:T(8,128)(2,1)S(1)} collective-permute-done((bf16[2,32,1024]{2,1,0:T(8,128)(2,1)S(1)}, bf16[2,32,1024]{2,1,0:T(8,128)(2,1)S(1)}, u32[]{:S(2)}, u32[]{:S(2)}) %collective-permute-start.33) | collective-permute-done | bytes 131104 | tf_op jit(solution)/shard_map/ppermute | solution.py:30
  87.6 3.4 %collective-permute-start.31 = (bf16[32,1152]{1,0:T(8,128)(2,1)S(1)}, bf16[32,1152]{1,0:T(8,128)(2,1)S(1)}, u32[]{:S(2)}, u32[]{:S(2)}) collective-permute-start(bf16[32,1152]{1,0:T(8,128)(2,1)S(1)} %fusion.14), channel_id=1, source_target_pairs={{0,16},{1,17},{2,18},{3,19},{4,20},{5,21},{6,22},{7,23},{8,24},{9,... | collective-permute-start | bytes 221192 | tf_op jit(solution)/shard_map/ppermute | solution.py:30
  93.7 2.2 %read.1 = bf16[32,512]{1,0:T(8,128)(2,1)S(1)} custom-call(f32[32,2176]{1,0:T(8,128)S(1)} %pad_maximum_fusion.sums_ref, f32[1,512]{1,0:T(1,128)S(1)} %bitcast.133, f32[1,128]{1,0:T(1,128)S(1)} %bitcast.139, f32[32,4,128,128]{3,2,1,0:T(8,128)S(1)} %bitcast.123), custom_call_target="tpu_custom_call" | custom-call | tf_op jit(solution)/shard_map/read/pallas_call | solution.py:280
  95.9 2.1 %collective-permute-start.37 = (bf16[32,512]{1,0:T(8,128)(2,1)S(1)}, bf16[32,512]{1,0:T(8,128)(2,1)S(1)}, u32[]{:S(2)}, u32[]{:S(2)}) collective-permute-start(bf16[32,512]{1,0:T(8,128)(2,1)S(1)} %read.1), channel_id=1, source_target_pairs={{0,24},{1,25},{2,26},{3,27},{4,28},{5,29},{6,30},{7,31},{8,16},{9,... | collective-permute-start | bytes 98312 | tf_op jit(solution)/shard_map/ppermute | solution.py:30
  104.2 4.1 %collective-permute-done.38.far = bf16[4,32,512]{2,1,0:T(8,128)(2,1)S(1)} collective-permute-done((bf16[4,32,512]{2,1,0:T(8,128)(2,1)S(1)}, bf16[4,32,512]{2,1,0:T(8,128)(2,1)S(1)}, u32[]{:S(2)}, u32[]{:S(2)}) %collective-permute-start.38) | collective-permute-done | bytes 131104 | tf_op jit(solution)/shard_map/ppermute | solution.py:30
  110.9 2.4 %collective-permute-done.39 = bf16[256,128]{1,0:T(8,128)(2,1)S(1)} collective-permute-done((bf16[256,128]{1,0:T(8,128)(2,1)S(1)}, bf16[256,128]{1,0:T(8,128)(2,1)S(1)}, u32[]{:S(2)}, u32[]{:S(2)}) %collective-permute-start.39) | collective-permute-done | bytes 65568 | tf_op jit(solution)/shard_map/ppermute | solution.py:30
  119.5 2.1 %collective-permute-start.52 = (bf16[128,128]{1,0:T(8,128)(2,1)S(1)}, bf16[128,128]{1,0:T(8,128)(2,1)S(1)}, u32[]{:S(2)}, u32[]{:S(2)}) collective-permute-start(bf16[128,128]{1,0:T(8,128)(2,1)S(1)} %get-tuple-element.96), channel_id=1, source_target_pairs={{0,8},{1,9},{2,10},{3,11},{4,12},{5,13},{6,14},{7,15},{8,0},{9,1},... | collective-permute-start | bytes 98312 | tf_op jit(solution)/shard_map/ppermute | solution.py:30
  130.7 2.4 %collective-permute-done.46.refs_2_ = bf16[4,128,128]{2,1,0:T(8,128)(2,1)S(1)} collective-permute-done((bf16[4,128,128]{2,1,0:T(8,128)(2,1)S(1)}, bf16[4,128,128]{2,1,0:T(8,128)(2,1)S(1)}, u32[]{:S(2)}, u32[]{:S(2)}) %collective-permute-start.46) | collective-permute-done | bytes 131104 | tf_op jit(solution)/shard_map/ppermute | solution.py:30
  140.6 3.8 %half_step.3 = (bf16[4,256,128]{2,1,0:T(8,128)(2,1)S(1)}, bf16[4,256,128]{2,1,0:T(8,128)(2,1)S(1)}, bf16[4,256,128]{2,1,0:T(8,128)(2,1)S(1)}, bf16[4,256,128]{2,...) custom-call(s32[1]{0:T(128)} %bitcast.me_ref, ...), custom_call_target="tpu_custom_call" | custom-call | tf_op jit(solution)/shard_map/half_step/pallas_call | solution.py:113
  144.8 3.1 %update.2.refs_0_ = f32[32,4,128,128]{3,2,1,0:T(8,128)} custom-call(f32[32,2176]{1,0:T(8,128)S(1)} %pad_maximum_fusion.sums_ref, f32[1,512]{1,0:T(1,128)S(1)} %bitcast.134, f32[32,4,128,128]{3,2,1,0:T(8,128)S(1)} %bitcast.123), custom_call_target="tpu_custom_call" | custom-call | flops 1000000000 | bytes 8388608 | tf_op jit(solution)/shard_map/update/pallas_call | solution.py:334
  147.9 3.1 %update.3 = f32[32,4,128,128]{3,2,1,0:T(8,128)} custom-call(f32[32,2176]{1,0:T(8,128)S(1)} %pad_maximum_fusion.sums_ref, f32[1,512]{1,0:T(1,128)S(1)} %bitcast.135, f32[32,4,128,128]{3,2,1,0:T(8,128)S(1)} %bitcast.123, f32[32,4,128,128]{3,2,1,0:T(8,128)} %update.2.refs_0_), custom_call_target="tpu_custom_call", output_to_operand_aliasing={{}: (3, {})} | custom-call | flops 1000000000 | bytes 8388608 | tf_op jit(solution)/shard_map/update/pallas_call | solution.py:334
  158.2 3.9 %collective-permute-done.64 = bf16[4,128,128]{2,1,0:T(8,128)(2,1)S(1)} collective-permute-done((bf16[4,128,128]{2,1,0:T(8,128)(2,1)S(1)}, bf16[4,128,128]{2,1,0:T(8,128)(2,1)S(1)}, u32[]{:S(2)}, u32[]{:S(2)}) %collective-permute-start.64) | collective-permute-done | bytes 131104 | tf_op jit(solution)/shard_map/ppermute | solution.py:30
  164.5 2.2 %collective-permute-start.71 = (bf16[128,128]{1,0:T(8,128)(2,1)S(1)}, bf16[128,128]{1,0:T(8,128)(2,1)S(1)}, u32[]{:S(2)}, u32[]{:S(2)}) collective-permute-start(bf16[128,128]{1,0:T(8,128)(2,1)S(1)} %get-tuple-element.83), channel_id=1, source_target_pairs={{0,24},{1,25},{2,26},{3,27},{4,28},{5,29},{6,30},{7,31},{8,16},{9,... | collective-permute-start | bytes 98312 | tf_op jit(solution)/shard_map/ppermute | solution.py:30
  169.1 2.1 %collective-permute-start.77 = (bf16[128,128]{1,0:T(8,128)(2,1)S(1)}, bf16[128,128]{1,0:T(8,128)(2,1)S(1)}, u32[]{:S(2)}, u32[]{:S(2)}) collective-permute-start(bf16[128,128]{1,0:T(8,128)(2,1)S(1)} %get-tuple-element.86), channel_id=1, source_target_pairs={{0,24},{1,25},{2,26},{3,27},{4,28},{5,29},{6,30},{7,31},{8,16},{9,... | collective-permute-start | bytes 98312 | tf_op jit(solution)/shard_map/ppermute | solution.py:30
  172.0 2.8 %collective-permute-done.77 = bf16[128,128]{1,0:T(8,128)(2,1)S(1)} collective-permute-done((bf16[128,128]{1,0:T(8,128)(2,1)S(1)}, bf16[128,128]{1,0:T(8,128)(2,1)S(1)}, u32[]{:S(2)}, u32[]{:S(2)}) %collective-permute-start.77) | collective-permute-done | bytes 32800 | tf_op jit(solution)/shard_map/ppermute | solution.py:30
  (236 shorter events, 94.6 us)
Async XLA Ops:
  0.6 7.9 %collective-permute-start.2 = (bf16[256,128]{1,0:T(8,128)(2,1)}, bf16[256,128]{1,0:T(8,128)(2,1)S(1)}, u32[]{:S(2)}, u32[]{:S(2)}) collective-permute-start(bf16[256,128]{1,0:T(8,128)(2,1)} %param.18), channel_id=1, source_target_pairs={{0,24},{1,25},{2,26},{3,27},{4,28},{5,29},{6,30},{7,31},{8,16},{9,... | collective-permute-start | bytes 196616 | tf_op jit(solution)/shard_map/ppermute | solution.py:30
  12.5 9.2 %collective-permute-start.5 = (bf16[4,256,128]{2,1,0:T(8,128)(2,1)S(1)}, bf16[4,256,128]{2,1,0:T(8,128)(2,1)S(1)}, u32[]{:S(2)}, u32[]{:S(2)}) collective-permute-start(bf16[4,256,128]{2,1,0:T(8,128)(2,1)S(1)} %pad_maximum_fusion.1.refs_0_), channel_id=1, source_target_pairs={{0,2},{1,3},{2,0},{3,1},{4,6},{5,7},{6,4},{7,5},{8,10},{9,11},{10,... | collective-permute-start | bytes 786440 | tf_op jit(solution)/shard_map/ppermute | solution.py:30
  14.0 13.3 %collective-permute-start.4 = (bf16[4,256,128]{2,1,0:T(8,128)(2,1)S(1)}, bf16[4,256,128]{2,1,0:T(8,128)(2,1)S(1)}, u32[]{:S(2)}, u32[]{:S(2)}) collective-permute-start(bf16[4,256,128]{2,1,0:T(8,128)(2,1)S(1)} %pad_maximum_fusion.1.refs_0_), channel_id=1, source_target_pairs={{0,4},{1,5},{2,6},{3,7},{4,0},{5,1},{6,2},{7,3},{8,12},{9,13},{10,... | collective-permute-start | bytes 786440 | tf_op jit(solution)/shard_map/ppermute | solution.py:30
  15.6 11.8 %collective-permute-start.3 = (bf16[4,256,128]{2,1,0:T(8,128)(2,1)S(1)}, bf16[4,256,128]{2,1,0:T(8,128)(2,1)S(1)}, u32[]{:S(2)}, u32[]{:S(2)}) collective-permute-start(bf16[4,256,128]{2,1,0:T(8,128)(2,1)S(1)} %pad_maximum_fusion.1.refs_0_), channel_id=1, source_target_pairs={{0,6},{1,7},{2,4},{3,5},{4,2},{5,3},{6,0},{7,1},{8,14},{9,15},{10,... | collective-permute-start | bytes 786440 | tf_op jit(solution)/shard_map/ppermute | solution.py:30
  16.0 17.3 %collective-permute-start.6 = (bf16[4,256,128]{2,1,0:T(8,128)(2,1)S(1)}, bf16[4,256,128]{2,1,0:T(8,128)(2,1)S(1)}, u32[]{:S(2)}, u32[]{:S(2)}) collective-permute-start(bf16[4,256,128]{2,1,0:T(8,128)(2,1)S(1)} %pad_maximum_fusion.1.refs_0_), channel_id=1, source_target_pairs={{0,1},{1,0},{2,3},{3,2},{4,5},{5,4},{6,7},{7,6},{8,9},{9,8},{10,11... | collective-permute-start | bytes 786440 | tf_op jit(solution)/shard_map/ppermute | solution.py:30
  21.7 11.6 %collective-permute-start.9 = (bf16[4,256,128]{2,1,0:T(8,128)(2,1)S(1)}, bf16[4,256,128]{2,1,0:T(8,128)(2,1)S(1)}, u32[]{:S(2)}, u32[]{:S(2)}) collective-permute-start(bf16[4,256,128]{2,1,0:T(8,128)(2,1)S(1)} %collective-permute-done.5.refs_3_), channel_id=1, source_target_pairs={{0,1},{1,0},{2,3},{3,2},{4,5},{5,4},{6,7},{7,6},{8,9},{9,8},{10,11... | collective-permute-start | bytes 786440 | tf_op jit(solution)/shard_map/ppermute | solution.py:30
  42.4 14.9 %collective-permute-start.20 = (bf16[4,128,128]{2,1,0:T(8,128)(2,1)S(1)}, bf16[4,128,128]{2,1,0:T(8,128)(2,1)S(1)}, u32[]{:S(2)}, u32[]{:S(2)}) collective-permute-start(bf16[4,128,128]{2,1,0:T(8,128)(2,1)S(1)} %get-tuple-element.76), channel_id=1, source_target_pairs={{0,6},{1,7},{2,4},{3,5},{4,2},{5,3},{6,0},{7,1},{8,14},{9,15},{10,... | collective-permute-start | bytes 393224 | tf_op jit(solution)/shard_map/ppermute | solution.py:30
  43.9 8.6 %collective-permute-start.12 = (bf16[4,128,128]{2,1,0:T(8,128)(2,1)S(1)}, bf16[4,128,128]{2,1,0:T(8,128)(2,1)S(1)}, u32[]{:S(2)}, u32[]{:S(2)}) collective-permute-start(bf16[4,128,128]{2,1,0:T(8,128)(2,1)S(1)} %get-tuple-element.77), channel_id=1, source_target_pairs={{0,6},{1,7},{2,4},{3,5},{4,2},{5,3},{6,0},{7,1},{8,14},{9,15},{10,... | collective-permute-start | bytes 393224 | tf_op jit(solution)/shard_map/ppermute | solution.py:30
  45.5 9.1 %collective-permute-start.14 = (bf16[4,128,128]{2,1,0:T(8,128)(2,1)S(1)}, bf16[4,128,128]{2,1,0:T(8,128)(2,1)S(1)}, u32[]{:S(2)}, u32[]{:S(2)}) collective-permute-start(bf16[4,128,128]{2,1,0:T(8,128)(2,1)S(1)} %get-tuple-element.78), channel_id=1, source_target_pairs={{0,4},{1,5},{2,6},{3,7},{4,0},{5,1},{6,2},{7,3},{8,12},{9,13},{10,... | collective-permute-start | bytes 393224 | tf_op jit(solution)/shard_map/ppermute | solution.py:30
  47.1 12.1 %collective-permute-start.21 = (bf16[4,128,128]{2,1,0:T(8,128)(2,1)S(1)}, bf16[4,128,128]{2,1,0:T(8,128)(2,1)S(1)}, u32[]{:S(2)}, u32[]{:S(2)}) collective-permute-start(bf16[4,128,128]{2,1,0:T(8,128)(2,1)S(1)} %get-tuple-element.79), channel_id=1, source_target_pairs={{0,4},{1,5},{2,6},{3,7},{4,0},{5,1},{6,2},{7,3},{8,12},{9,13},{10,... | collective-permute-start | bytes 393224 | tf_op jit(solution)/shard_map/ppermute | solution.py:30
  47.7 7.7 %collective-permute-start.16 = (bf16[4,128,128]{2,1,0:T(8,128)(2,1)S(1)}, bf16[4,128,128]{2,1,0:T(8,128)(2,1)S(1)}, u32[]{:S(2)}, u32[]{:S(2)}) collective-permute-start(bf16[4,128,128]{2,1,0:T(8,128)(2,1)S(1)} %get-tuple-element.80), channel_id=1, source_target_pairs={{0,2},{1,3},{2,0},{3,1},{4,6},{5,7},{6,4},{7,5},{8,10},{9,11},{10,... | collective-permute-start | bytes 393224 | tf_op jit(solution)/shard_map/ppermute | solution.py:30
  72.9 8.4 %collective-permute-start.32 = (bf16[2,2,32,1024]{3,2,0,1:T(8,128)(2,1)S(1)}, bf16[2,2,32,1024]{3,2,0,1:T(8,128)(2,1)S(1)}, u32[]{:S(2)}, u32[]{:S(2)}) collective-permute-start(bf16[2,2,32,1024]{3,2,0,1:T(8,128)(2,1)S(1)} %bitcast.141), channel_id=1, source_target_pairs={{0,8},{1,9},{2,10},{3,11},{4,12},{5,13},{6,14},{7,15},{8,0},{9,1},... | collective-permute-start | bytes 786440 | tf_op jit(solution)/shard_map/ppermute | solution.py:30
  73.2 8.9 %collective-permute-start.29 = (bf16[2,2,32,1152]{3,2,0,1:T(8,128)(2,1)S(1)}, bf16[2,2,32,1152]{3,2,0,1:T(8,128)(2,1)S(1)}, u32[]{:S(2)}, u32[]{:S(2)}) collective-permute-start(bf16[2,2,32,1152]{3,2,0,1:T(8,128)(2,1)S(1)} %bitcast.140), channel_id=1, source_target_pairs={{0,4},{1,5},{2,6},{3,7},{4,0},{5,1},{6,2},{7,3},{8,12},{9,13},{10,... | collective-permute-start | bytes 884744 | tf_op jit(solution)/shard_map/ppermute | solution.py:30
  114.3 7.3 %collective-permute-start.43 = (bf16[128,128]{1,0:T(8,128)(2,1)S(1)}, bf16[128,128]{1,0:T(8,128)(2,1)S(1)}, u32[]{:S(2)}, u32[]{:S(2)}) collective-permute-start(bf16[128,128]{1,0:T(8,128)(2,1)S(1)} %get-tuple-element.97), channel_id=1, source_target_pairs={{0,16},{1,17},{2,18},{3,19},{4,20},{5,21},{6,22},{7,23},{8,24},{9,... | collective-permute-start | bytes 98312 | tf_op jit(solution)/shard_map/ppermute | solution.py:30
  124.5 8.7 %collective-permute-start.46 = (bf16[4,128,128]{2,1,0:T(8,128)(2,1)S(1)}, bf16[4,128,128]{2,1,0:T(8,128)(2,1)S(1)}, u32[]{:S(2)}, u32[]{:S(2)}) collective-permute-start(bf16[4,128,128]{2,1,0:T(8,128)(2,1)S(1)} %pad_maximum_fusion.3.refs_0_), channel_id=1, source_target_pairs={{0,4},{1,5},{2,6},{3,7},{4,0},{5,1},{6,2},{7,3},{8,12},{9,13},{10,... | collective-permute-start | bytes 393224 | tf_op jit(solution)/shard_map/ppermute | solution.py:30
  125.2 8.7 %collective-permute-start.45 = (bf16[4,128,128]{2,1,0:T(8,128)(2,1)S(1)}, bf16[4,128,128]{2,1,0:T(8,128)(2,1)S(1)}, u32[]{:S(2)}, u32[]{:S(2)}) collective-permute-start(bf16[4,128,128]{2,1,0:T(8,128)(2,1)S(1)} %pad_maximum_fusion.3.refs_0_), channel_id=1, source_target_pairs={{0,6},{1,7},{2,4},{3,5},{4,2},{5,3},{6,0},{7,1},{8,14},{9,15},{10,... | collective-permute-start | bytes 393224 | tf_op jit(solution)/shard_map/ppermute | solution.py:30
  127.4 7.9 %collective-permute-start.57 = (bf16[4,128,128]{2,1,0:T(8,128)(2,1)S(1)}, bf16[4,128,128]{2,1,0:T(8,128)(2,1)S(1)}, u32[]{:S(2)}, u32[]{:S(2)}) collective-permute-start(bf16[4,128,128]{2,1,0:T(8,128)(2,1)S(1)} %pad_maximum_fusion.4.refs_8_), channel_id=1, source_target_pairs={{0,2},{1,3},{2,0},{3,1},{4,6},{5,7},{6,4},{7,5},{8,10},{9,11},{10,... | collective-permute-start | bytes 393224 | tf_op jit(solution)/shard_map/ppermute | solution.py:30
  129.7 7.4 %collective-permute-start.56 = (bf16[4,128,128]{2,1,0:T(8,128)(2,1)S(1)}, bf16[4,128,128]{2,1,0:T(8,128)(2,1)S(1)}, u32[]{:S(2)}, u32[]{:S(2)}) collective-permute-start(bf16[4,128,128]{2,1,0:T(8,128)(2,1)S(1)} %pad_maximum_fusion.4.refs_8_), channel_id=1, source_target_pairs={{0,4},{1,5},{2,6},{3,7},{4,0},{5,1},{6,2},{7,3},{8,12},{9,13},{10,... | collective-permute-start | bytes 393224 | tf_op jit(solution)/shard_map/ppermute | solution.py:30
  144.4 7.4 %collective-permute-start.63 = (bf16[4,256,128]{2,1,0:T(8,128)(2,1)S(1)}, bf16[4,256,128]{2,1,0:T(8,128)(2,1)S(1)}, u32[]{:S(2)}, u32[]{:S(2)}) collective-permute-start(bf16[4,256,128]{2,1,0:T(8,128)(2,1)S(1)} %get-tuple-element.51), channel_id=1, source_target_pairs={{0,1},{1,0},{2,3},{3,2},{4,5},{5,4},{6,7},{7,6},{8,9},{9,8},{10,11... | collective-permute-start | bytes 786440 | tf_op jit(solution)/shard_map/ppermute | solution.py:30
  151.9 14.8 %collective-permute-start.72 = (bf16[4,128,128]{2,1,0:T(8,128)(2,1)S(1)}, bf16[4,128,128]{2,1,0:T(8,128)(2,1)S(1)}, u32[]{:S(2)}, u32[]{:S(2)}) collective-permute-start(bf16[4,128,128]{2,1,0:T(8,128)(2,1)S(1)} %get-tuple-element.70), channel_id=1, source_target_pairs={{0,6},{1,7},{2,4},{3,5},{4,2},{5,3},{6,0},{7,1},{8,14},{9,15},{10,... | collective-permute-start | bytes 393224 | tf_op jit(solution)/shard_map/ppermute | solution.py:30
  153.0 9.0 %collective-permute-start.64 = (bf16[4,128,128]{2,1,0:T(8,128)(2,1)S(1)}, bf16[4,128,128]{2,1,0:T(8,128)(2,1)S(1)}, u32[]{:S(2)}, u32[]{:S(2)}) collective-permute-start(bf16[4,128,128]{2,1,0:T(8,128)(2,1)S(1)} %get-tuple-element.71), channel_id=1, source_target_pairs={{0,6},{1,7},{2,4},{3,5},{4,2},{5,3},{6,0},{7,1},{8,14},{9,15},{10,... | collective-permute-start | bytes 393224 | tf_op jit(solution)/shard_map/ppermute | solution.py:30
  154.9 9.3 %collective-permute-start.66 = (bf16[4,128,128]{2,1,0:T(8,128)(2,1)S(1)}, bf16[4,128,128]{2,1,0:T(8,128)(2,1)S(1)}, u32[]{:S(2)}, u32[]{:S(2)}) collective-permute-start(bf16[4,128,128]{2,1,0:T(8,128)(2,1)S(1)} %get-tuple-element.72), channel_id=1, source_target_pairs={{0,4},{1,5},{2,6},{3,7},{4,0},{5,1},{6,2},{7,3},{8,12},{9,13},{10,... | collective-permute-start | bytes 393224 | tf_op jit(solution)/shard_map/ppermute | solution.py:30
  155.1 12.8 %collective-permute-start.73 = (bf16[4,128,128]{2,1,0:T(8,128)(2,1)S(1)}, bf16[4,128,128]{2,1,0:T(8,128)(2,1)S(1)}, u32[]{:S(2)}, u32[]{:S(2)}) collective-permute-start(bf16[4,128,128]{2,1,0:T(8,128)(2,1)S(1)} %get-tuple-element.73), channel_id=1, source_target_pairs={{0,4},{1,5},{2,6},{3,7},{4,0},{5,1},{6,2},{7,3},{8,12},{9,13},{10,... | collective-permute-start | bytes 393224 | tf_op jit(solution)/shard_map/ppermute | solution.py:30
  164.5 7.1 %collective-permute-start.71 = (bf16[128,128]{1,0:T(8,128)(2,1)S(1)}, bf16[128,128]{1,0:T(8,128)(2,1)S(1)}, u32[]{:S(2)}, u32[]{:S(2)}) collective-permute-start(bf16[128,128]{1,0:T(8,128)(2,1)S(1)} %get-tuple-element.83), channel_id=1, source_target_pairs={{0,24},{1,25},{2,26},{3,27},{4,28},{5,29},{6,30},{7,31},{8,16},{9,... | collective-permute-start | bytes 98312 | tf_op jit(solution)/shard_map/ppermute | solution.py:30
  (76 other events, 755.7 us)
